TPU v7x, 256 devices: a whole 4x4x8 slice. The times are simulated.
256 devices in a mesh: tp: 16 (over y, x), dp: 16 (over z, core).
Axes of the slice: x: 4, y: 4, z: 8, core: 2. Of those that a mesh axis runs over, the one named last changes fastest.
Arguments:
- tokens: bfloat16 [256, 4096], P(None, 'dp'), may hold values from -15 to 15, as said below
- norm_gain: float32 [2, 4096], P(None, 'dp'), may hold values from 0.1 to 1.9
- w_query: bfloat16 [2, 4096, 2048], P(None, 'dp', 'tp'), may hold values from -0.09375 to 0.09375
- w_forget: bfloat16 [2, 4096, 2048], P(None, 'dp', 'tp'), may hold values from -0.09375 to 0.09375
- w_value: bfloat16 [2, 4096, 2048], P(None, 'dp', 'tp'), may hold values from -0.09375 to 0.09375
- w_gate: bfloat16 [2, 4096, 2048], P(None, 'dp', 'tp'), may hold values from -0.09375 to 0.09375
- floor_rate: float32 [2, 2048], P(None, 'tp'), may hold values from 0 to 0.9
- head_gain: float32 [2, 128], replicated, may hold values from 0.1 to 1.9
- w_output: bfloat16 [2, 2048, 4096], P(None, 'tp', 'dp'), may hold values from -0.3 to 0.3
- state: float32 [2, 256, 16, 128, 128], P(None, 'dp', 'tp'), may hold values from -4 to 4
Outputs:
- mixed: bfloat16 [256, 4096], P(None, 'dp')
- new_state: float32 [2, 256, 16, 128, 128], P(None, 'dp', 'tp')
Inputs may be any that keep to these rules, and one draw needn't show every extreme that they name: `tokens`: activations whose feature blocks have different scales.
All inputs are finite; a program needn't handle non-finite values.
Results may differ from a plain program's by a relative error of at most 0.035.
Values may be sent and summed in bfloat16 or wider, within the bound.
No kernel may reach another device: no remote copies, remote signals or barrier semaphores. Data moves between devices by JAX's collectives and lax.ppermute only.
A program may use at most 64 MiB of HBM per device.

v0:
```python
import functools

import jax
import jax.numpy as jnp
from jax import lax
from jax.experimental import pallas as pl
from jax.experimental.pallas import tpu as pltpu
from jax.sharding import Mesh
from jax.sharding import PartitionSpec as P


D = 4096
EPS = 1e-06
BF16 = jnp.bfloat16
F32 = jnp.float32
LANES = 128


START_LIMIT = 56 * 2**20


def call(kernel, outs, *args, flops=0):
    vmem = pl.BlockSpec(memory_space=pltpu.VMEM)
    size = sum(a.size * a.dtype.itemsize for a in args)
    return pl.pallas_call(
        kernel,
        out_shape=outs,
        in_specs=[vmem] * len(args),
        out_specs=[vmem] * len(outs),
        cost_estimate=pl.CostEstimate(flops=flops, bytes_accessed=size, transcendentals=0),
        compiler_params=pltpu.CompilerParams(vmem_limit_bytes=12 * 2**20),
    )(*args)


def rounded(x):
    return x.astype(BF16).astype(F32)


def project(x, gain, weights):
    x = x.astype(F32)
    normed = (x * gain).astype(BF16)
    products = [jnp.dot(normed, w, preferred_element_type=F32) for w in weights]
    return products, jnp.sum(x * x, axis=1, keepdims=True)


def in_three(squares):
    high = rounded(squares)
    middle = rounded(squares - high)
    low = squares - high - middle
    lane = lax.broadcasted_iota(jnp.int32, (squares.shape[0], LANES), 1)
    return jnp.where(
        lane == 0, high, jnp.where(lane == 1, middle, jnp.where(lane == 2, low, 0.0))
    )


def store(totals, squares, payload_ref):
    n_z, own_rows, _ = payload_ref.shape
    for p, part in enumerate([*totals, in_three(squares)]):
        payload_ref[:, :, p * LANES : (p + 1) * LANES] = (
            part.astype(BF16).reshape(n_z, own_rows, LANES)
        )


def start_kernel(tok, gain, floor_rate, head_gain, *refs):
    w = refs[0:4]
    keep_ref, send_ref, bundle_ref, tok_here, gain_here, rates_here, w_here, sems = refs[4:]
    core = lax.axis_index("c")
    n_z, _, own_rows, feats = tok.shape
    rows = n_z * own_rows
    copies = [
        pltpu.make_async_copy(tok, tok_here, sems.at[0]),
        pltpu.make_async_copy(gain, gain_here, sems.at[1]),
        pltpu.make_async_copy(floor_rate, rates_here.at[0], sems.at[2]),
        pltpu.make_async_copy(head_gain, rates_here.at[1], sems.at[3]),
        *[pltpu.make_async_copy(w[p], w_here.at[p], sems.at[4 + p]) for p in range(4)],
    ]
    for copy in copies:
        copy.start()
    for copy in copies:
        copy.wait()
    weights = [w_here.at[p] for p in range(4)]
    gain_0 = gain_here[0:1, :]
    x = tok_here[:, 1 - core].reshape(rows, feats)
    bundle_ref[0:rows, 4 * LANES :] = x
    store(*project(x, gain_0, [v[0] for v in weights]), send_ref)
    x = tok_here[:, core].reshape(rows, feats)
    totals, squares = project(x, gain_0, [v[0] for v in weights])
    for p in range(4):
        keep_ref[0:rows, p * LANES : (p + 1) * LANES] = totals[p]
        bundle_ref[0:feats, p * LANES : (p + 1) * LANES] = weights[p][1]
    keep_ref[0:rows, 4 * LANES :] = in_three(squares)
    keep_ref[rows : rows + 2, 0:LANES] = rates_here[0]
    keep_ref[rows + 2 : rows + 4, 0:LANES] = rates_here[1]
    gain_1 = gain_here[1:2, :]
    high = rounded(gain_1)
    middle = rounded(gain_1 - high)
    for n, term in enumerate((high, middle, gain_1 - high - middle)):
        bundle_ref[rows + 16 * n : rows + 16 * n + 16, 4 * LANES :] = jnp.broadcast_to(
            term, (16, feats)
        ).astype(BF16)


def start(payload_shape, rows, *own):
    vmem = pl.BlockSpec(memory_space=pltpu.VMEM)
    hbm = pl.BlockSpec(memory_space=pltpu.HBM)
    feats = own[1].shape[1]
    return pl.pallas_call(
        start_kernel,
        out_shape=[
            jax.ShapeDtypeStruct((rows + 8, 5 * LANES), F32),
            payload_shape,
            jax.ShapeDtypeStruct((feats, 4 * LANES + feats), BF16),
        ],
        in_specs=[hbm] * len(own),
        out_specs=[vmem] * 3,
        scratch_shapes=[
            pltpu.VMEM(own[0].shape, BF16),
            pltpu.VMEM(own[1].shape, F32),
            pltpu.VMEM((2, *own[2].shape), F32),
            pltpu.VMEM((4, *own[4].shape), BF16),
            pltpu.SemaphoreType.DMA((8,)),
        ],
        cost_estimate=pl.CostEstimate(flops=10**8, bytes_accessed=10**6, transcendentals=0),
        compiler_params=pltpu.CompilerParams(vmem_limit_bytes=START_LIMIT),
        name="start",
    )(*own)


def pair_kernel(keep, received, payload_ref, rates_ref):
    n_z, own_rows, width = received.shape
    rates_ref[...] = keep[n_z * own_rows :, 0:LANES]
    total = keep[0 : n_z * own_rows, :] + received[...].reshape(n_z * own_rows, width).astype(F32)
    extra = total[:, 4 * LANES :]
    squares = extra[:, 0:1] + extra[:, 1:2] + extra[:, 2:3]
    store([total[:, p * LANES : (p + 1) * LANES] for p in range(4)], squares, payload_ref)


def add_up(parts, halves):
    terms = [p[...].astype(F32) for p in parts]
    update = (terms[0] + terms[1]) + (terms[2] + terms[3])
    feats = halves[0].shape[1]
    return [
        (half.astype(F32) + update[:, n * feats : (n + 1) * feats]).astype(BF16)
        for n, half in enumerate(halves)
    ]


def middle_kernel(p0, p1, p2, p3, tok, bundle_a, bundle_b, payload_ref, x_ref):
    core = lax.axis_index("c")
    n_z, _, own_rows, feats = tok.shape
    rows = n_z * own_rows
    mine = tok[:, core].reshape(rows, feats)
    halves = add_up((p0, p1, p2, p3), [mine, bundle_b[0:rows, 4 * LANES :]])
    results = []
    for half, bundle in zip(halves, (bundle_a, bundle_b)):
        gain = sum(
            bundle[rows + 16 * n : rows + 16 * n + 16, 4 * LANES :][0:1].astype(F32)
            for n in range(3)
        )
        weights = [bundle[:, p * LANES : (p + 1) * LANES] for p in range(4)]
        results.append(project(half, gain, weights))
    (totals, squares), (others, other_squares) = results
    store([t + o for t, o in zip(totals, others)], squares + other_squares, payload_ref)
    x_ref[0] = halves[0]
    x_ref[1] = halves[1]


def last_kernel(*refs):
    parts, (x_in, keep_ref, send_ref) = refs[0:4], refs[4:]
    halves = add_up(parts, [x_in[0], x_in[1]])
    keep_ref[...] = halves[0]
    send_ref[...] = halves[1]


def join_kernel(keep, received, out_ref):
    core = lax.axis_index("c")
    n_z, _, own_rows, feats = out_ref.shape
    out_ref[:, core] = keep[...].reshape(n_z, own_rows, feats)
    out_ref[:, 1 - core] = received[...].reshape(n_z, own_rows, feats)


def sigmoid(x):
    return 1.0 / (1.0 + jnp.exp(-x))


def mix_kernel(layer, arrived, rates, state, gated_ref, terms_ref):
    summed = arrived[0].astype(F32)
    for n in range(1, arrived.shape[0]):
        summed = summed + arrived[n].astype(F32)
    own_rows = summed.shape[0]
    extra = summed[:, 4 * LANES :]
    square = extra[:, 0:1] + extra[:, 1:2] + extra[:, 2:3]
    row_scale = lax.rsqrt(square / D + EPS)
    query_pre, forget_pre, value, gate_pre = [
        row_scale * summed[:, p * LANES : (p + 1) * LANES] for p in range(4)
    ]
    floor = rates[layer : layer + 1, :]
    query = query_pre * sigmoid(query_pre) * LANES ** (-0.5)
    forget = floor + (1.0 - floor) * sigmoid(forget_pre)
    key_in = (1.0 - floor) * sigmoid(-forget_pre)
    terms_ref[0] = forget
    terms_ref[1] = key_in
    terms_ref[2] = value
    columns = (query * forget).T
    fresh = jnp.sum(query * key_in, axis=1, keepdims=True) * value
    kept = [
        jnp.sum(state[layer, i, 0] * columns[:, i : i + 1], axis=0, keepdims=True)
        for i in range(own_rows)
    ]
    read = jnp.concatenate(kept, axis=0) + fresh
    read = read * lax.rsqrt(jnp.mean(read * read, axis=1, keepdims=True) + EPS)
    gate = gate_pre * sigmoid(gate_pre)
    gated = (read * rates[layer + 2 : layer + 3, :] * gate).astype(BF16)
    for n in range(gated_ref.shape[0]):
        gated_ref[n] = gated


def update_kernel(terms_a, terms_b, state, out_ref):
    def write(terms):
        forget = terms[0].T
        key_in = terms[1].T
        for i in range(state.shape[1]):
            value = terms[2, i : i + 1, :]
            out_ref[0, i, 0] = state[0, i, 0] * forget[:, i : i + 1] + key_in[:, i : i + 1] * value

    @pl.when(pl.program_id(0) == 0)
    def _():
        write(terms_a)

    @pl.when(pl.program_id(0) == 1)
    def _():
        write(terms_b)


def new_states(terms_a, terms_b, state):
    layers, seqs, heads, dk, dv = state.shape
    step = 8
    terms_spec = pl.BlockSpec((3, step, dk), lambda l, i: (0, i, 0))
    state_spec = pl.BlockSpec((1, step, heads, dk, dv), lambda l, i: (l, i, 0, 0, 0))
    return pl.pallas_call(
        update_kernel,
        out_shape=jax.ShapeDtypeStruct(state.shape, F32),
        grid=(layers, seqs // step),
        in_specs=[terms_spec, terms_spec, state_spec],
        out_specs=state_spec,
        cost_estimate=pl.CostEstimate(flops=10**7, bytes_accessed=2 * state.size * 4, transcendentals=0),
        compiler_params=pltpu.CompilerParams(vmem_limit_bytes=12 * 2**20),
        name="new_states",
    )(terms_a, terms_b, state)


def output_kernel(layer, heads, w_a, w_b, out_ref):
    my_x = lax.axis_index("x")
    n_x = heads.shape[0]
    rows = heads.shape[1] * heads.shape[2]
    for half, w in enumerate((w_a, w_b)):
        total = None
        for i in range(n_x):
            block = w[lax.rem(my_x - i + n_x, n_x), layer]
            product = jnp.dot(
                heads[i].reshape(rows, LANES), block, preferred_element_type=F32
            )
            total = product if total is None else total + product
        total = total.astype(BF16)
        feats = total.shape[1]
        out_ref[:, half * feats : (half + 1) * feats] = total


def spread(copies, axes):
    return lax.all_to_all(copies, axes, split_axis=0, concat_axis=0, tiled=True)


def per_device(
    tokens, norm_gain, w_query, w_forget, w_value, w_gate, floor_rate, head_gain, w_output, state
):
    n_z, n_x, n_y = lax.axis_size("z"), lax.axis_size("x"), lax.axis_size("y")
    batch, feats = tokens.shape
    own_rows = batch // (2 * n_z)
    rows = n_z * own_rows

    def swap(v):
        return lax.ppermute(v, "c", [(0, 1), (1, 0)])

    weights = (w_query, w_forget, w_value, w_gate)
    tok = tokens.reshape(n_z, 2, own_rows, feats)
    payload_shape = jax.ShapeDtypeStruct((n_z, own_rows, 5 * LANES), BF16)
    x_shape = jax.ShapeDtypeStruct((2, rows, feats), BF16)
    keep, send, bundle = start(
        payload_shape, rows, tok, norm_gain, floor_rate, head_gain, *weights
    )
    received = swap(send)
    payload, rates = call(
        pair_kernel, [payload_shape, jax.ShapeDtypeStruct((8, LANES), F32)],
        keep, received, flops=10**6,
    )
    bundle_b = swap(bundle)
    pieces = [w_output]
    for k in range(1, n_x):
        pieces.append(lax.ppermute(w_output, "x", [(i, (i + k) % n_x) for i in range(n_x)]))
    gathered = jnp.stack(pieces)
    w_out = (gathered, swap(gathered))

    terms = []
    for layer in range(2):
        arrived = spread(payload, "z")
        gated, term = call(
            functools.partial(mix_kernel, layer),
            [
                jax.ShapeDtypeStruct((n_x * n_z, own_rows, LANES), BF16),
                jax.ShapeDtypeStruct((3, own_rows, LANES), F32),
            ],
            arrived, rates, state, flops=10**7,
        )
        terms.append(term)
        heads = spread(gated, ("x", "z")).reshape(n_x, n_z, own_rows, LANES)
        (own,) = call(
            functools.partial(output_kernel, layer),
            [jax.ShapeDtypeStruct((rows, 2 * feats), BF16)],
            heads, *w_out, flops=10**8,
        )
        parts = [own]
        for k in range(1, n_y):
            parts.append(lax.ppermute(own, "y", [(i, i ^ k) for i in range(n_y)]))
        if layer == 0:
            payload, x = call(
                middle_kernel, [payload_shape, x_shape],
                *parts, tok, bundle, bundle_b, flops=10**8,
            )
    half = jax.ShapeDtypeStruct((rows, feats), BF16)
    keep, send = call(last_kernel, [half, half], *parts, x, flops=10**6)
    states = new_states(*terms, state)
    received = swap(send)
    (mixed,) = call(
        join_kernel, [jax.ShapeDtypeStruct((n_z, 2, own_rows, feats), BF16)],
        keep, received, flops=10**6,
    )
    return mixed.reshape(batch, feats), states


def solution(mesh):
    n_tp, n_dp = mesh.devices.shape
    fine = Mesh(mesh.devices.reshape(4, n_tp // 4, n_dp // 2, 2), ("y", "x", "z", "c"))
    dp, tp = ("z", "c"), ("y", "x")
    in_specs = (
        P(None, dp),
        P(None, dp),
        P(None, dp, tp),
        P(None, dp, tp),
        P(None, dp, tp),
        P(None, dp, tp),
        P(None, tp),
        P(),
        P(None, tp, dp),
        P(None, dp, tp, None, None),
    )
    out_specs = (P(None, dp), P(None, dp, tp, None, None))
    return jax.shard_map(
        per_device, mesh=fine, in_specs=in_specs, out_specs=out_specs, check_vma=False
    )
```

profile of v0, /device:TPU:1, one launch (start us, length us, event | category | flops | bytes accessed | tf_op | source)
XLA Modules:
  0.0 96.3 jit_solution(15265490192336177365)
XLA Ops:
  0.6 0.0 copy-start
  0.6 2.6 %start.1 = (f32[136,640]{1,0:T(8,128)}, bf16[8,16,640]{2,1,0:T(8,128)(2,1)}, bf16[256,768]{1,0:T(8,128)(2,1)}) custom-call(bf16[8,2,16,256]{3,2,1,0:T(8,128)(2,1)} %bitcast.10, f32[2,256]{1,0:T(2,128)} %gain.1, f32[2,128]{1,0:T(2,128)} %floor_rate.1, f32[2,128]{1,0:T(2,128)} %head_gain.1, bf16[2,256,128]{2,1,0:T(8,128)(2,1)} %refs_0_.1, ...), custom_call_target="tpu_custom_call" | custom-call | flops 100000000 | bytes 1000000 | tf_op jit(solution)/shard_map/start/pallas_call | solution.py:107
  3.2 3.3 %collective-permute-start = (bf16[8,16,640]{2,1,0:T(8,128)(2,1)}, bf16[8,16,640]{2,1,0:T(8,128)(2,1)S(1)}, u32[]{:S(2)}, u32[]{:S(2)}) collective-permute-start(bf16[8,16,640]{2,1,0:T(8,128)(2,1)} %get-tuple-element.16), channel_id=1, source_target_pairs={{0,1},{1,0},{2,3},{3,2},{4,5},{5,4},{6,7},{7,6},{8,9},{9,8},{10,11... | collective-permute-start | bytes 491528 | tf_op jit(solution)/shard_map/ppermute | solution.py:282
  6.5 0.0 collective-permute-start.1
  6.5 2.7 %collective-permute-start.3 = (bf16[2,128,256]{2,1,0:T(8,128)(2,1)}, bf16[2,128,256]{2,1,0:T(8,128)(2,1)S(1)}, u32[]{:S(2)}, u32[]{:S(2)}) collective-permute-start(bf16[2,128,256]{2,1,0:T(8,128)(2,1)} %param.18), channel_id=1, source_target_pairs={{0,48},{16,0},{32,16},{48,32},{1,49},{17,1},{33,17},{49,33},{2,50}... | collective-permute-start | bytes 393224 | tf_op jit(solution)/shard_map/ppermute | solution.py:299
  9.2 0.0 collective-permute-start.2
  9.2 0.0 collective-permute-done.received
  9.2 0.0 copy-start.3
  9.2 1.0 %copy-done.3 = f32[136,640]{1,0:T(8,128)S(1)} copy-done((f32[136,640]{1,0:T(8,128)S(1)}, f32[136,640]{1,0:T(8,128)}, u32[]{:S(2)}) %copy-start.3) | copy-done | bytes 348184
  10.2 0.9 shard_map.113
  11.0 8.0 %all-to-all-start = ((bf16[8,16,640]{2,1,0:T(8,128)(2,1)}), bf16[8,16,640]{2,1,0:T(8,128)(2,1)S(1)}, u32[]{:S(2)}, u32[]{:S(2)}) async-start(bf16[8,16,640]{2,1,0:T(8,128)(2,1)} %get-tuple-element.17), calls=%async_computation | async-start | bytes 327680 | tf_op jit(solution)/shard_map/all_to_all | solution.py:270
  19.0 0.0 collective-permute-done.1
  19.0 0.0 collective-permute-done.3
  19.1 0.0 collective-permute-done.2
  19.1 1.0 %pad_maximum_fusion.w_a = bf16[4,2,128,256]{3,2,1,0:T(8,128)(2,1)S(1)} fusion(bf16[1,2,128,256]{3,2,1,0:T(8,128)(2,1)S(1)} %bitcast.15, bf16[1,2,128,256]{3,2,1,0:T(8,128)(2,1)S(1)} %bitcast.16, bf16[1,2,128,256]{3,2,1,0:T(8,128)(2,1)S(1)} %bitcast.14, bf16[1,2,128,256]{3,2,1,0:T(8,128)(2,1)} %bitcast.13), kind=kLoop, calls=%fused_computation | loop fusion | flops 786432 | bytes 1048576 | tf_op jit(solution)/shard_map/stack | solution.py:300
  20.0 0.0 copy-start.1
  20.1 1.3 %collective-permute-start.4 = (bf16[4,2,128,256]{3,2,1,0:T(8,128)(2,1)S(1)}, bf16[4,2,128,256]{3,2,1,0:T(8,128)(2,1)S(1)}, u32[]{:S(2)}, u32[]{:S(2)}) collective-permute-start(bf16[4,2,128,256]{3,2,1,0:T(8,128)(2,1)S(1)} %pad_maximum_fusion.w_a), channel_id=1, source_target_pairs={{0,1},{1,0},{2,3},{3,2},{4,5},{5,4},{6,7},{7,6},{8,9},{9,8},{10,11... | collective-permute-start | bytes 1572872 | tf_op jit(solution)/shard_map/ppermute | solution.py:282
  21.3 5.8 %all-to-all-done.arrived = bf16[8,16,640]{2,1,0:T(8,128)(2,1)S(1)} async-done(((bf16[8,16,640]{2,1,0:T(8,128)(2,1)}), bf16[8,16,640]{2,1,0:T(8,128)(2,1)S(1)}, u32[]{:S(2)}, u32[]{:S(2)}) %all-to-all-start) | async-done | bytes 163872 | tf_op jit(solution)/shard_map/all_to_all | solution.py:270
  27.1 0.0 copy-done
  27.1 0.7 shard_map.114
  27.9 0.0 copy-start.4
  27.9 0.6 copy-done.4
  28.5 3.9 %all-to-all-start.1 = ((bf16[32,16,128]{2,1,0:T(8,128)(2,1)}), bf16[32,16,128]{2,1,0:T(8,128)(2,1)S(1)}, u32[]{:S(2)}, u32[]{:S(2)}) async-start(bf16[32,16,128]{2,1,0:T(8,128)(2,1)} %copy-done.4), calls=%async_computation.1 | async-start | bytes 262144 | tf_op jit(solution)/shard_map/all_to_all | solution.py:270
  32.4 2.7 %collective-permute-start.8 = (bf16[256,768]{1,0:T(8,128)(2,1)}, bf16[256,768]{1,0:T(8,128)(2,1)}, u32[]{:S(2)}, u32[]{:S(2)}) collective-permute-start(bf16[256,768]{1,0:T(8,128)(2,1)} %get-tuple-element.20.bundle_a), channel_id=1, source_target_pairs={{0,1},{1,0},{2,3},{3,2},{4,5},{5,4},{6,7},{7,6},{8,9},{9,8},{10,11... | collective-permute-start | bytes 1179656 | tf_op jit(solution)/shard_map/ppermute | solution.py:282
  35.1 0.0 collective-permute-done.4.w_b
  35.1 6.5 %all-to-all-done.1 = bf16[32,16,128]{2,1,0:T(8,128)(2,1)S(1)} async-done(((bf16[32,16,128]{2,1,0:T(8,128)(2,1)}), bf16[32,16,128]{2,1,0:T(8,128)(2,1)S(1)}, u32[]{:S(2)}, u32[]{:S(2)}) %all-to-all-start.1) | async-done | bytes 131104 | tf_op jit(solution)/shard_map/all_to_all | solution.py:270
  41.6 0.3 shard_map.115.p0
  41.9 2.8 %collective-permute-start.7 = (bf16[128,512]{1,0:T(8,128)(2,1)S(1)}, bf16[128,512]{1,0:T(8,128)(2,1)S(1)}, u32[]{:S(2)}, u32[]{:S(2)}) collective-permute-start(bf16[128,512]{1,0:T(8,128)(2,1)S(1)} %shard_map.115.p0), channel_id=1, source_target_pairs={{0,192},{64,128},{128,64},{192,0},{1,193},{65,129},{129,65},{193,1... | collective-permute-start | bytes 393224 | tf_op jit(solution)/shard_map/ppermute | solution.py:323
  44.7 0.4 collective-permute-start.6
  45.1 0.3 collective-permute-start.5
  45.4 0.0 collective-permute-done.8.bundle_b
  45.4 2.6 %collective-permute-done.7.p3 = bf16[128,512]{1,0:T(8,128)(2,1)S(1)} collective-permute-done((bf16[128,512]{1,0:T(8,128)(2,1)S(1)}, bf16[128,512]{1,0:T(8,128)(2,1)S(1)}, u32[]{:S(2)}, u32[]{:S(2)}) %collective-permute-start.7) | collective-permute-done | bytes 131104 | tf_op jit(solution)/shard_map/ppermute | solution.py:323
  48.0 2.0 %collective-permute-done.6.p2 = bf16[128,512]{1,0:T(8,128)(2,1)S(1)} collective-permute-done((bf16[128,512]{1,0:T(8,128)(2,1)S(1)}, bf16[128,512]{1,0:T(8,128)(2,1)S(1)}, u32[]{:S(2)}, u32[]{:S(2)}) %collective-permute-start.6) | collective-permute-done | bytes 131104 | tf_op jit(solution)/shard_map/ppermute | solution.py:323
  50.1 0.0 collective-permute-done.5.p1
  50.1 0.0 copy-done.1
  50.1 0.0 copy-start.2
  50.1 1.0 %copy-done.2 = bf16[256,768]{1,0:T(8,128)(2,1)S(1)} copy-done((bf16[256,768]{1,0:T(8,128)(2,1)S(1)}, bf16[256,768]{1,0:T(8,128)(2,1)}, u32[]{:S(2)}) %copy-start.2) | copy-done | bytes 393240
  51.1 1.3 %shard_map.116 = (bf16[8,16,640]{2,1,0:T(8,128)(2,1)S(1)}, bf16[2,128,256]{2,1,0:T(8,128)(2,1)S(1)}) custom-call(bf16[128,512]{1,0:T(8,128)(2,1)S(1)} %shard_map.115.p0, bf16[128,512]{1,0:T(8,128)(2,1)S(1)} %collective-permute-done.5.p1, bf16[128,512]{1,0:T(8,128)(2,1)S(1)} %collective-permute-done.6.p2, bf16[128,512]{1,0:T(8,128)(2,1)S(1)} %collective-permute-done.7.p3, ...), custom_call_target="tpu_custom_call" | custom-call | flops 100000000 | bytes 1441792 | tf_op jit(solution)/shard_map/pallas_call | solution.py:25
  52.4 10.7 %all_to_all.20.arrived = bf16[8,16,640]{2,1,0:T(8,128)(2,1)S(1)} all-to-all(bf16[8,16,640]{2,1,0:T(8,128)(2,1)S(1)} %get-tuple-element.21), channel_id=1, replica_groups=mesh['y'=4,'x'=4,'z'=8,'c'=2] {'z'}, dimensions={0} | all-to-all | bytes 327680 | tf_op jit(solution)/shard_map/all_to_all | solution.py:270
  63.1 0.7 shard_map.117
  63.8 12.1 %all_to_all.21 = bf16[32,16,128]{2,1,0:T(8,128)(2,1)S(1)} all-to-all(bf16[32,16,128]{2,1,0:T(8,128)(2,1)S(1)} %get-tuple-element.22), channel_id=1, replica_groups=mesh['y'=4,'x'=4,'z'=8,'c'=2] {'x','z'}, dimensions={0} | all-to-all | bytes 262144 | tf_op jit(solution)/shard_map/all_to_all | solution.py:270
  75.9 0.3 shard_map.118.refs_0_
  76.2 1.8 %collective-permute-start.11 = (bf16[128,512]{1,0:T(8,128)(2,1)S(1)}, bf16[128,512]{1,0:T(8,128)(2,1)S(1)}, u32[]{:S(2)}, u32[]{:S(2)}) collective-permute-start(bf16[128,512]{1,0:T(8,128)(2,1)S(1)} %shard_map.118.refs_0_), channel_id=1, source_target_pairs={{0,192},{64,128},{128,64},{192,0},{1,193},{65,129},{129,65},{193,1... | collective-permute-start | bytes 393224 | tf_op jit(solution)/shard_map/ppermute | solution.py:323
  78.0 0.7 collective-permute-start.10
  78.6 0.9 collective-permute-start.9
  79.5 2.1 %collective-permute-done.11.refs_3_ = bf16[128,512]{1,0:T(8,128)(2,1)S(1)} collective-permute-done((bf16[128,512]{1,0:T(8,128)(2,1)S(1)}, bf16[128,512]{1,0:T(8,128)(2,1)S(1)}, u32[]{:S(2)}, u32[]{:S(2)}) %collective-permute-start.11) | collective-permute-done | bytes 131104 | tf_op jit(solution)/shard_map/ppermute | solution.py:323
  81.6 1.7 %collective-permute-done.10.refs_2_ = bf16[128,512]{1,0:T(8,128)(2,1)S(1)} collective-permute-done((bf16[128,512]{1,0:T(8,128)(2,1)S(1)}, bf16[128,512]{1,0:T(8,128)(2,1)S(1)}, u32[]{:S(2)}, u32[]{:S(2)}) %collective-permute-start.10) | collective-permute-done | bytes 131104 | tf_op jit(solution)/shard_map/ppermute | solution.py:323
  83.3 0.1 collective-permute-done.9.refs_1_
  83.4 0.1 shard_map.119
  83.4 9.0 %collective-permute-start.12 = (bf16[128,256]{1,0:T(8,128)(2,1)S(1)}, bf16[128,256]{1,0:T(8,128)(2,1)S(1)}, u32[]{:S(2)}, u32[]{:S(2)}) collective-permute-start(bf16[128,256]{1,0:T(8,128)(2,1)S(1)} %get-tuple-element.25), channel_id=1, source_target_pairs={{0,1},{1,0},{2,3},{3,2},{4,5},{5,4},{6,7},{7,6},{8,9},{9,8},{10,11... | collective-permute-start | bytes 196616 | tf_op jit(solution)/shard_map/ppermute | solution.py:282
  92.5 3.2 %new_states.1 = f32[2,16,1,128,128]{4,3,2,1,0:T(8,128)} custom-call(f32[3,16,128]{2,1,0:T(8,128)S(1)} %get-tuple-element.26.terms_a, f32[3,16,128]{2,1,0:T(8,128)S(1)} %get-tuple-element.27.terms_b, f32[2,16,1,128,128]{4,3,2,1,0:T(8,128)S(1)} %copy-done), custom_call_target="tpu_custom_call" | custom-call | flops 10000000 | bytes 4194304 | tf_op jit(solution)/shard_map/new_states/pallas_call | solution.py:240
  95.6 0.0 collective-permute-done.12.received
  95.6 0.7 shard_map.120
Async XLA Ops:
  0.6 26.5 %copy-start = (f32[2,16,1,128,128]{4,3,2,1,0:T(8,128)S(1)}, f32[2,16,1,128,128]{4,3,2,1,0:T(8,128)}, u32[]{:S(2)}) copy-start(f32[2,16,1,128,128]{4,3,2,1,0:T(8,128)} %state.5) | copy-start | bytes 6291460
  3.2 6.0 %collective-permute-start = (bf16[8,16,640]{2,1,0:T(8,128)(2,1)}, bf16[8,16,640]{2,1,0:T(8,128)(2,1)S(1)}, u32[]{:S(2)}, u32[]{:S(2)}) collective-permute-start(bf16[8,16,640]{2,1,0:T(8,128)(2,1)} %get-tuple-element.16), channel_id=1, source_target_pairs={{0,1},{1,0},{2,3},{3,2},{4,5},{5,4},{6,7},{7,6},{8,9},{9,8},{10,11... | collective-permute-start | bytes 491528 | tf_op jit(solution)/shard_map/ppermute | solution.py:282
  6.5 12.5 %collective-permute-start.1 = (bf16[2,128,256]{2,1,0:T(8,128)(2,1)}, bf16[2,128,256]{2,1,0:T(8,128)(2,1)S(1)}, u32[]{:S(2)}, u32[]{:S(2)}) collective-permute-start(bf16[2,128,256]{2,1,0:T(8,128)(2,1)} %param.18), channel_id=1, source_target_pairs={{0,16},{16,32},{32,48},{48,0},{1,17},{17,33},{33,49},{49,1},{2,18}... | collective-permute-start | bytes 393224 | tf_op jit(solution)/shard_map/ppermute | solution.py:299
  6.5 12.5 %collective-permute-start.3 = (bf16[2,128,256]{2,1,0:T(8,128)(2,1)}, bf16[2,128,256]{2,1,0:T(8,128)(2,1)S(1)}, u32[]{:S(2)}, u32[]{:S(2)}) collective-permute-start(bf16[2,128,256]{2,1,0:T(8,128)(2,1)} %param.18), channel_id=1, source_target_pairs={{0,48},{16,0},{32,16},{48,32},{1,49},{17,1},{33,17},{49,33},{2,50}... | collective-permute-start | bytes 393224 | tf_op jit(solution)/shard_map/ppermute | solution.py:299
  9.2 9.9 %collective-permute-start.2 = (bf16[2,128,256]{2,1,0:T(8,128)(2,1)}, bf16[2,128,256]{2,1,0:T(8,128)(2,1)S(1)}, u32[]{:S(2)}, u32[]{:S(2)}) collective-permute-start(bf16[2,128,256]{2,1,0:T(8,128)(2,1)} %param.18), channel_id=1, source_target_pairs={{0,32},{16,48},{32,0},{48,16},{1,33},{17,49},{33,1},{49,17},{2,34}... | collective-permute-start | bytes 393224 | tf_op jit(solution)/shard_map/ppermute | solution.py:299
  9.2 1.0 %copy-start.3 = (f32[136,640]{1,0:T(8,128)S(1)}, f32[136,640]{1,0:T(8,128)}, u32[]{:S(2)}) copy-start(f32[136,640]{1,0:T(8,128)} %get-tuple-element.15.keep) | copy-start | bytes 1044484
  11.0 16.1 %all-to-all-start = ((bf16[8,16,640]{2,1,0:T(8,128)(2,1)}), bf16[8,16,640]{2,1,0:T(8,128)(2,1)S(1)}, u32[]{:S(2)}, u32[]{:S(2)}) async-start(bf16[8,16,640]{2,1,0:T(8,128)(2,1)} %get-tuple-element.17), calls=%async_computation | async-start | bytes 327680 | tf_op jit(solution)/shard_map/all_to_all | solution.py:270
  20.0 30.0 %copy-start.1 = (bf16[256,256]{1,0:T(8,128)(2,1)S(1)}, bf16[256,256]{1,0:T(8,128)(2,1)}, u32[]{:S(2)}) copy-start(bf16[256,256]{1,0:T(8,128)(2,1)} %param.10) | copy-start | bytes 393220
  20.1 15.1 %collective-permute-start.4 = (bf16[4,2,128,256]{3,2,1,0:T(8,128)(2,1)S(1)}, bf16[4,2,128,256]{3,2,1,0:T(8,128)(2,1)S(1)}, u32[]{:S(2)}, u32[]{:S(2)}) collective-permute-start(bf16[4,2,128,256]{3,2,1,0:T(8,128)(2,1)S(1)} %pad_maximum_fusion.w_a), channel_id=1, source_target_pairs={{0,1},{1,0},{2,3},{3,2},{4,5},{5,4},{6,7},{7,6},{8,9},{9,8},{10,11... | collective-permute-start | bytes 1572872 | tf_op jit(solution)/shard_map/ppermute | solution.py:282
  27.9 0.7 copy-start.4
  28.5 13.1 %all-to-all-start.1 = ((bf16[32,16,128]{2,1,0:T(8,128)(2,1)}), bf16[32,16,128]{2,1,0:T(8,128)(2,1)S(1)}, u32[]{:S(2)}, u32[]{:S(2)}) async-start(bf16[32,16,128]{2,1,0:T(8,128)(2,1)} %copy-done.4), calls=%async_computation.1 | async-start | bytes 262144 | tf_op jit(solution)/shard_map/all_to_all | solution.py:270
  32.4 13.0 %collective-permute-start.8 = (bf16[256,768]{1,0:T(8,128)(2,1)}, bf16[256,768]{1,0:T(8,128)(2,1)}, u32[]{:S(2)}, u32[]{:S(2)}) collective-permute-start(bf16[256,768]{1,0:T(8,128)(2,1)} %get-tuple-element.20.bundle_a), channel_id=1, source_target_pairs={{0,1},{1,0},{2,3},{3,2},{4,5},{5,4},{6,7},{7,6},{8,9},{9,8},{10,11... | collective-permute-start | bytes 1179656 | tf_op jit(solution)/shard_map/ppermute | solution.py:282
  41.9 6.1 %collective-permute-start.7 = (bf16[128,512]{1,0:T(8,128)(2,1)S(1)}, bf16[128,512]{1,0:T(8,128)(2,1)S(1)}, u32[]{:S(2)}, u32[]{:S(2)}) collective-permute-start(bf16[128,512]{1,0:T(8,128)(2,1)S(1)} %shard_map.115.p0), channel_id=1, source_target_pairs={{0,192},{64,128},{128,64},{192,0},{1,193},{65,129},{129,65},{193,1... | collective-permute-start | bytes 393224 | tf_op jit(solution)/shard_map/ppermute | solution.py:323
  44.7 5.3 %collective-permute-start.6 = (bf16[128,512]{1,0:T(8,128)(2,1)S(1)}, bf16[128,512]{1,0:T(8,128)(2,1)S(1)}, u32[]{:S(2)}, u32[]{:S(2)}) collective-permute-start(bf16[128,512]{1,0:T(8,128)(2,1)S(1)} %shard_map.115.p0), channel_id=1, source_target_pairs={{0,128},{64,192},{128,0},{192,64},{1,129},{65,193},{129,1},{193,65... | collective-permute-start | bytes 393224 | tf_op jit(solution)/shard_map/ppermute | solution.py:323
  45.1 5.0 %collective-permute-start.5 = (bf16[128,512]{1,0:T(8,128)(2,1)S(1)}, bf16[128,512]{1,0:T(8,128)(2,1)S(1)}, u32[]{:S(2)}, u32[]{:S(2)}) collective-permute-start(bf16[128,512]{1,0:T(8,128)(2,1)S(1)} %shard_map.115.p0), channel_id=1, source_target_pairs={{0,64},{64,0},{128,192},{192,128},{1,65},{65,1},{129,193},{193,129... | collective-permute-start | bytes 393224 | tf_op jit(solution)/shard_map/ppermute | solution.py:323
  50.1 1.0 %copy-start.2 = (bf16[256,768]{1,0:T(8,128)(2,1)S(1)}, bf16[256,768]{1,0:T(8,128)(2,1)}, u32[]{:S(2)}) copy-start(bf16[256,768]{1,0:T(8,128)(2,1)} %get-tuple-element.20.bundle_a) | copy-start | bytes 1179652
  76.2 5.4 %collective-permute-start.11 = (bf16[128,512]{1,0:T(8,128)(2,1)S(1)}, bf16[128,512]{1,0:T(8,128)(2,1)S(1)}, u32[]{:S(2)}, u32[]{:S(2)}) collective-permute-start(bf16[128,512]{1,0:T(8,128)(2,1)S(1)} %shard_map.118.refs_0_), channel_id=1, source_target_pairs={{0,192},{64,128},{128,64},{192,0},{1,193},{65,129},{129,65},{193,1... | collective-permute-start | bytes 393224 | tf_op jit(solution)/shard_map/ppermute | solution.py:323
  78.0 5.3 %collective-permute-start.10 = (bf16[128,512]{1,0:T(8,128)(2,1)S(1)}, bf16[128,512]{1,0:T(8,128)(2,1)S(1)}, u32[]{:S(2)}, u32[]{:S(2)}) collective-permute-start(bf16[128,512]{1,0:T(8,128)(2,1)S(1)} %shard_map.118.refs_0_), channel_id=1, source_target_pairs={{0,128},{64,192},{128,0},{192,64},{1,129},{65,193},{129,1},{193,65... | collective-permute-start | bytes 393224 | tf_op jit(solution)/shard_map/ppermute | solution.py:323
  78.6 4.7 %collective-permute-start.9 = (bf16[128,512]{1,0:T(8,128)(2,1)S(1)}, bf16[128,512]{1,0:T(8,128)(2,1)S(1)}, u32[]{:S(2)}, u32[]{:S(2)}) collective-permute-start(bf16[128,512]{1,0:T(8,128)(2,1)S(1)} %shard_map.118.refs_0_), channel_id=1, source_target_pairs={{0,64},{64,0},{128,192},{192,128},{1,65},{65,1},{129,193},{193,129... | collective-permute-start | bytes 393224 | tf_op jit(solution)/shard_map/ppermute | solution.py:323
  83.4 12.2 %collective-permute-start.12 = (bf16[128,256]{1,0:T(8,128)(2,1)S(1)}, bf16[128,256]{1,0:T(8,128)(2,1)S(1)}, u32[]{:S(2)}, u32[]{:S(2)}) collective-permute-start(bf16[128,256]{1,0:T(8,128)(2,1)S(1)} %get-tuple-element.25), channel_id=1, source_target_pairs={{0,1},{1,0},{2,3},{3,2},{4,5},{5,4},{6,7},{7,6},{8,9},{9,8},{10,11... | collective-permute-start | bytes 196616 | tf_op jit(solution)/shard_map/ppermute | solution.py:282
where the time goes:
time: 96.8 us; the launch traced here: 96.3 us
  starting transfers between devices  37.7 us (39%)
  blocking collectives  22.8 us (24%)
  waiting for transfers between devices  20.7 us (21%)
  Pallas kernels  10.7 us (11%)
  local copies, waits for them, and re-layouts  2.63 us (3%)
  other arithmetic  0.97 us (1%)
    all_to_all x2, blocking collectives, spread(): return lax.all_to_all(copies, axes, split_axis=0, concat_axis=0, tiled=True)  22.8 us
    ppermute x4, starting transfers between devices, swap(): return lax.ppermute(v, 'c', [(0, 1), (1, 0)])  16.4 us
    all_to_all x2, waiting for transfers between devices, spread(): return lax.all_to_all(copies, axes, split_axis=0, concat_axis=0, tiled=True)  12.3 us
    all_to_all x2, starting transfers between devices, spread(): return lax.all_to_all(copies, axes, split_axis=0, concat_axis=0, tiled=True)  11.9 us
    ppermute x6, waiting for transfers between devices, per_device(): parts.append(lax.ppermute(own, 'y', [(i, i ^ k) for i in range(n_y)]))  8.46 us
    ppermute x6, starting transfers between devices, per_device(): parts.append(lax.ppermute(own, 'y', [(i, i ^ k) for i in range(n_y)]))  6.81 us
    pallas_call x8, Pallas kernels, call(): pl.pallas_call(kernel, out_shape=outs, in_specs=[vmem] * len(args), out_s...  4.97 us
    pallas_call x1, Pallas kernels, new_states(): pl.pallas_call(update_kernel, out_shape=jax.ShapeDtypeStruct(state.shape,...  3.17 us
  transfers between devices with their start and end apart: 15, of which 7 were waited for; matrix products, arithmetic and copies ran while one was open for 1% of the time, Pallas kernels for 5%

commit v1 on v0

--- a/solution.py
+++ b/solution.py
@@ -61,36 +61,27 @@
         )
 
 
-def start_kernel(tok, gain, floor_rate, head_gain, *refs):
+def start_kernel(tok, gain, *refs):
     w = refs[0:4]
-    keep_ref, send_ref, bundle_ref, tok_here, gain_here, rates_here, w_here, sems = refs[4:]
+    payload_ref, bundle_ref, tok_here, gain_here, w_here, sems = refs[4:]
     core = lax.axis_index("c")
     n_z, _, own_rows, feats = tok.shape
     rows = n_z * own_rows
     copies = [
         pltpu.make_async_copy(tok, tok_here, sems.at[0]),
         pltpu.make_async_copy(gain, gain_here, sems.at[1]),
-        pltpu.make_async_copy(floor_rate, rates_here.at[0], sems.at[2]),
-        pltpu.make_async_copy(head_gain, rates_here.at[1], sems.at[3]),
-        *[pltpu.make_async_copy(w[p], w_here.at[p], sems.at[4 + p]) for p in range(4)],
+        *[pltpu.make_async_copy(w[p], w_here.at[p], sems.at[2 + p]) for p in range(4)],
     ]
     for copy in copies:
         copy.start()
     for copy in copies:
         copy.wait()
     weights = [w_here.at[p] for p in range(4)]
-    gain_0 = gain_here[0:1, :]
-    x = tok_here[:, 1 - core].reshape(rows, feats)
-    bundle_ref[0:rows, 4 * LANES :] = x
-    store(*project(x, gain_0, [v[0] for v in weights]), send_ref)
-    x = tok_here[:, core].reshape(rows, feats)
-    totals, squares = project(x, gain_0, [v[0] for v in weights])
+    x = tok_here[...].reshape(2 * rows, feats)
+    store(*project(x, gain_here[0:1, :], [v[0] for v in weights]), payload_ref)
     for p in range(4):
-        keep_ref[0:rows, p * LANES : (p + 1) * LANES] = totals[p]
-        bundle_ref[0:feats, p * LANES : (p + 1) * LANES] = weights[p][1]
-    keep_ref[0:rows, 4 * LANES :] = in_three(squares)
-    keep_ref[rows : rows + 2, 0:LANES] = rates_here[0]
-    keep_ref[rows + 2 : rows + 4, 0:LANES] = rates_here[1]
+        bundle_ref[:, p * LANES : (p + 1) * LANES] = weights[p][1]
+    bundle_ref[0:rows, 4 * LANES :] = tok_here[:, 1 - core].reshape(rows, feats)
     gain_1 = gain_here[1:2, :]
     high = rounded(gain_1)
     middle = rounded(gain_1 - high)
@@ -100,25 +91,23 @@
         ).astype(BF16)
 
 
-def start(payload_shape, rows, *own):
+def start(n_dp, own_rows, *own):
     vmem = pl.BlockSpec(memory_space=pltpu.VMEM)
     hbm = pl.BlockSpec(memory_space=pltpu.HBM)
     feats = own[1].shape[1]
     return pl.pallas_call(
         start_kernel,
         out_shape=[
-            jax.ShapeDtypeStruct((rows + 8, 5 * LANES), F32),
-            payload_shape,
+            jax.ShapeDtypeStruct((n_dp, own_rows, 5 * LANES), BF16),
             jax.ShapeDtypeStruct((feats, 4 * LANES + feats), BF16),
         ],
         in_specs=[hbm] * len(own),
-        out_specs=[vmem] * 3,
+        out_specs=[vmem] * 2,
         scratch_shapes=[
             pltpu.VMEM(own[0].shape, BF16),
             pltpu.VMEM(own[1].shape, F32),
-            pltpu.VMEM((2, *own[2].shape), F32),
-            pltpu.VMEM((4, *own[4].shape), BF16),
-            pltpu.SemaphoreType.DMA((8,)),
+            pltpu.VMEM((4, *own[2].shape), BF16),
+            pltpu.SemaphoreType.DMA((6,)),
         ],
         cost_estimate=pl.CostEstimate(flops=10**8, bytes_accessed=10**6, transcendentals=0),
         compiler_params=pltpu.CompilerParams(vmem_limit_bytes=START_LIMIT),
@@ -126,13 +115,9 @@
     )(*own)
 
 
-def pair_kernel(keep, received, payload_ref, rates_ref):
-    n_z, own_rows, width = received.shape
-    rates_ref[...] = keep[n_z * own_rows :, 0:LANES]
-    total = keep[0 : n_z * own_rows, :] + received[...].reshape(n_z * own_rows, width).astype(F32)
-    extra = total[:, 4 * LANES :]
-    squares = extra[:, 0:1] + extra[:, 1:2] + extra[:, 2:3]
-    store([total[:, p * LANES : (p + 1) * LANES] for p in range(4)], squares, payload_ref)
+def rates_kernel(floor_rate, head_gain, out_ref):
+    out_ref[0:2] = floor_rate[...]
+    out_ref[2:4] = head_gain[...]
 
 
 def add_up(parts, halves):
@@ -145,21 +130,19 @@
     ]
 
 
-def middle_kernel(p0, p1, p2, p3, tok, bundle_a, bundle_b, payload_ref, x_ref):
+def middle_kernel(p0, p1, p2, p3, tok, gain, *refs):
+    w, (bundle, payload_ref, x_ref) = refs[0:4], refs[4:]
     core = lax.axis_index("c")
     n_z, _, own_rows, feats = tok.shape
     rows = n_z * own_rows
     mine = tok[:, core].reshape(rows, feats)
-    halves = add_up((p0, p1, p2, p3), [mine, bundle_b[0:rows, 4 * LANES :]])
-    results = []
-    for half, bundle in zip(halves, (bundle_a, bundle_b)):
-        gain = sum(
-            bundle[rows + 16 * n : rows + 16 * n + 16, 4 * LANES :][0:1].astype(F32)
-            for n in range(3)
-        )
-        weights = [bundle[:, p * LANES : (p + 1) * LANES] for p in range(4)]
-        results.append(project(half, gain, weights))
-    (totals, squares), (others, other_squares) = results
+    halves = add_up((p0, p1, p2, p3), [mine, bundle[0:rows, 4 * LANES :]])
+    other_gain = sum(
+        bundle[rows + 16 * n : rows + 16 * n + 16, 4 * LANES :][0:1].astype(F32) for n in range(3)
+    )
+    totals, squares = project(halves[0], gain[1:2, :], [v[1] for v in w])
+    other_w = [bundle[:, p * LANES : (p + 1) * LANES] for p in range(4)]
+    others, other_squares = project(halves[1], other_gain, other_w)
     store([t + o for t, o in zip(totals, others)], squares + other_squares, payload_ref)
     x_ref[0] = halves[0]
     x_ref[1] = halves[1]
@@ -285,13 +268,10 @@
     tok = tokens.reshape(n_z, 2, own_rows, feats)
     payload_shape = jax.ShapeDtypeStruct((n_z, own_rows, 5 * LANES), BF16)
     x_shape = jax.ShapeDtypeStruct((2, rows, feats), BF16)
-    keep, send, bundle = start(
-        payload_shape, rows, tok, norm_gain, floor_rate, head_gain, *weights
-    )
-    received = swap(send)
-    payload, rates = call(
-        pair_kernel, [payload_shape, jax.ShapeDtypeStruct((8, LANES), F32)],
-        keep, received, flops=10**6,
+    payload, bundle = start(2 * n_z, own_rows, tok, norm_gain, *weights)
+    (rates,) = call(
+        rates_kernel, [jax.ShapeDtypeStruct((8, LANES), F32)],
+        floor_rate, head_gain, flops=10**4,
     )
     bundle_b = swap(bundle)
     pieces = [w_output]
@@ -302,7 +282,7 @@
 
     terms = []
     for layer in range(2):
-        arrived = spread(payload, "z")
+        arrived = spread(payload, ("z", "c") if layer == 0 else "z")
         gated, term = call(
             functools.partial(mix_kernel, layer),
             [
@@ -324,7 +304,7 @@
         if layer == 0:
             payload, x = call(
                 middle_kernel, [payload_shape, x_shape],
-                *parts, tok, bundle, bundle_b, flops=10**8,
+                *parts, tok, norm_gain, *weights, bundle_b, flops=10**8,
             )
     half = jax.ShapeDtypeStruct((rows, feats), BF16)
     keep, send = call(last_kernel, [half, half], *parts, x, flops=10**6)

time: 96.8 us -> 102 us (1.054)
  waiting for transfers between devices: 20.7 us -> 24.8 us
  local copies, waits for them, and re-layouts: 2.63 us -> 5.19 us
  starting transfers between devices: 37.7 us -> 36.6 us
    ppermute x4 -> x3, starting transfers between devices: 16.4 us -> 7.1 us  [swap(): return lax.ppermute(v, 'c', [(0, 1), (1, 0)])]
    ppermute x3, waiting for transfers between devices: 0.01 us -> 5.88 us  [per_device(): lax.ppermute(w_output, 'x', [(i, (i + k) % n_x) for i in range(n_x)])]
    all_to_all x2, starting transfers between devices: 11.9 us -> 17.6 us  [spread(): return lax.all_to_all(copies, axes, split_axis=0, concat_axis=0, tiled=True)]
    all_to_all x2, waiting for transfers between devices: 12.3 us -> 9.5 us  [spread(): return lax.all_to_all(copies, axes, split_axis=0, concat_axis=0, tiled=True)]
    unnamed x10 -> x20, local copies, waits for them, and re-layouts: 2.63 us -> 5.19 us
    ppermute x3, starting transfers between devices: 2.68 us -> 4.21 us  [per_device(): lax.ppermute(w_output, 'x', [(i, (i + k) % n_x) for i in range(n_x)])]
    all_to_all x2, blocking collectives: 22.8 us -> 23.8 us  [spread(): return lax.all_to_all(copies, axes, split_axis=0, concat_axis=0, tiled=True)]
  transfers between devices with their start and end apart: 15 -> 14, of which waited for: 7 -> 8; matrix products, arithmetic and copies ran while one was open for 1% -> 1% of each run, Pallas kernels for 5% -> 4%
where the time goes in v1:
time: 102 us
  starting transfers between devices  36.6 us (36%)
  waiting for transfers between devices  24.8 us (24%)
  blocking collectives  23.8 us (23%)
  Pallas kernels  9.83 us (10%)
  local copies, waits for them, and re-layouts  5.19 us (5%)
    all_to_all x2, blocking collectives, spread(): return lax.all_to_all(copies, axes, split_axis=0, concat_axis=0, tiled=True)  23.8 us
    all_to_all x2, starting transfers between devices, spread(): return lax.all_to_all(copies, axes, split_axis=0, concat_axis=0, tiled=True)  17.6 us
    all_to_all x2, waiting for transfers between devices, spread(): return lax.all_to_all(copies, axes, split_axis=0, concat_axis=0, tiled=True)  9.5 us
    ppermute x6, waiting for transfers between devices, per_device(): parts.append(lax.ppermute(own, 'y', [(i, i ^ k) for i in range(n_y)]))  9.39 us
    ppermute x6, starting transfers between devices, per_device(): parts.append(lax.ppermute(own, 'y', [(i, i ^ k) for i in range(n_y)]))  7.68 us
    ppermute x3, starting transfers between devices, swap(): return lax.ppermute(v, 'c', [(0, 1), (1, 0)])  7.1 us
    ppermute x3, waiting for transfers between devices, per_device(): lax.ppermute(w_output, 'x', [(i, (i + k) % n_x) for i in range(n_x)])  5.88 us
    unnamed x20, local copies, waits for them, and re-layouts  5.19 us
  transfers between devices with their start and end apart: 14, of which 8 were waited for; matrix products, arithmetic and copies ran while one was open for 1% of the time, Pallas kernels for 4%

profile of v1, /device:TPU:1, one launch (start us, length us, event | category | flops | bytes accessed | tf_op | source)
XLA Modules:
  0.0 101.9 jit_solution(11356702415384451823)
XLA Ops:
  0.6 0.0 copy-start.9
  0.6 0.0 copy-start.8
  0.7 0.0 copy-start
  0.7 2.5 %start.1 = (bf16[16,16,640]{2,1,0:T(8,128)(2,1)}, bf16[256,768]{1,0:T(8,128)(2,1)}) custom-call(bf16[8,2,16,256]{3,2,1,0:T(8,128)(2,1)} %bitcast.8, f32[2,256]{1,0:T(2,128)} %gain.3, bf16[2,256,128]{2,1,0:T(8,128)(2,1)} %refs_0_.3, bf16[2,256,128]{2,1,0:T(8,128)(2,1)} %refs_1_.3, bf16[2,256,128]{2,1,0:T(8,128)(2,1)} %refs_2_.3, bf16[2,256,128]{2,1,0:T(8,128)(2,1)} %refs_3_.3), custom_call_target="tpu_custom_call" | custom-call | flops 100000000 | bytes 1000000 | tf_op jit(solution)/shard_map/start/pallas_call | solution.py:98
  3.2 10.0 %all-to-all-start = ((bf16[16,16,640]{2,1,0:T(8,128)(2,1)}), bf16[16,16,640]{2,1,0:T(8,128)(2,1)S(1)}, u32[]{:S(2)}, u32[]{:S(2)}) async-start(bf16[16,16,640]{2,1,0:T(8,128)(2,1)} %get-tuple-element.12), calls=%async_computation | async-start | bytes 655360 | tf_op jit(solution)/shard_map/all_to_all | solution.py:253
  13.2 1.2 %collective-permute-start = (bf16[2,128,256]{2,1,0:T(8,128)(2,1)}, bf16[2,128,256]{2,1,0:T(8,128)(2,1)S(1)}, u32[]{:S(2)}, u32[]{:S(2)}) collective-permute-start(bf16[2,128,256]{2,1,0:T(8,128)(2,1)} %param.18), channel_id=1, source_target_pairs={{0,16},{16,32},{32,48},{48,0},{1,17},{17,33},{33,49},{49,1},{2,18}... | collective-permute-start | bytes 393224 | tf_op jit(solution)/shard_map/ppermute | solution.py:279
  14.4 1.5 %collective-permute-start.2 = (bf16[2,128,256]{2,1,0:T(8,128)(2,1)}, bf16[2,128,256]{2,1,0:T(8,128)(2,1)S(1)}, u32[]{:S(2)}, u32[]{:S(2)}) collective-permute-start(bf16[2,128,256]{2,1,0:T(8,128)(2,1)} %param.18), channel_id=1, source_target_pairs={{0,48},{16,0},{32,16},{48,32},{1,49},{17,1},{33,17},{49,33},{2,50}... | collective-permute-start | bytes 393224 | tf_op jit(solution)/shard_map/ppermute | solution.py:279
  15.8 1.5 %collective-permute-start.1 = (bf16[2,128,256]{2,1,0:T(8,128)(2,1)}, bf16[2,128,256]{2,1,0:T(8,128)(2,1)S(1)}, u32[]{:S(2)}, u32[]{:S(2)}) collective-permute-start(bf16[2,128,256]{2,1,0:T(8,128)(2,1)} %param.18), channel_id=1, source_target_pairs={{0,32},{16,48},{32,0},{48,16},{1,33},{17,49},{33,1},{49,17},{2,34}... | collective-permute-start | bytes 393224 | tf_op jit(solution)/shard_map/ppermute | solution.py:279
  17.4 2.1 %collective-permute-done = bf16[2,128,256]{2,1,0:T(8,128)(2,1)S(1)} collective-permute-done((bf16[2,128,256]{2,1,0:T(8,128)(2,1)}, bf16[2,128,256]{2,1,0:T(8,128)(2,1)S(1)}, u32[]{:S(2)}, u32[]{:S(2)}) %collective-permute-start) | collective-permute-done | bytes 131104 | tf_op jit(solution)/shard_map/ppermute | solution.py:279
  19.5 0.0 collective-permute-done.2
  19.5 3.8 %collective-permute-done.1 = bf16[2,128,256]{2,1,0:T(8,128)(2,1)S(1)} collective-permute-done((bf16[2,128,256]{2,1,0:T(8,128)(2,1)}, bf16[2,128,256]{2,1,0:T(8,128)(2,1)S(1)}, u32[]{:S(2)}, u32[]{:S(2)}) %collective-permute-start.1) | collective-permute-done | bytes 131104 | tf_op jit(solution)/shard_map/ppermute | solution.py:279
  23.3 1.0 pad_maximum_fusion.w_a
  24.2 0.0 copy-start.7
  24.2 1.1 %collective-permute-start.3 = (bf16[4,2,128,256]{3,2,1,0:T(8,128)(2,1)S(1)}, bf16[4,2,128,256]{3,2,1,0:T(8,128)(2,1)S(1)}, u32[]{:S(2)}, u32[]{:S(2)}) collective-permute-start(bf16[4,2,128,256]{3,2,1,0:T(8,128)(2,1)S(1)} %pad_maximum_fusion.w_a), channel_id=1, source_target_pairs={{0,1},{1,0},{2,3},{3,2},{4,5},{5,4},{6,7},{7,6},{8,9},{9,8},{10,11... | collective-permute-start | bytes 1572872 | tf_op jit(solution)/shard_map/ppermute | solution.py:265
  25.4 0.0 copy-done.9
  25.4 0.0 copy-done.8
  25.4 0.8 all-to-all-done.arrived
  26.1 0.0 copy-done
  26.1 0.8 shard_map.114
  26.9 0.0 copy-start.6
  26.9 0.6 copy-done.6
  27.6 7.6 %all-to-all-start.1 = ((bf16[32,16,128]{2,1,0:T(8,128)(2,1)}), bf16[32,16,128]{2,1,0:T(8,128)(2,1)S(1)}, u32[]{:S(2)}, u32[]{:S(2)}) async-start(bf16[32,16,128]{2,1,0:T(8,128)(2,1)} %copy-done.6), calls=%async_computation.1 | async-start | bytes 262144 | tf_op jit(solution)/shard_map/all_to_all | solution.py:253
  35.2 0.4 collective-permute-start.7
  35.6 0.0 collective-permute-done.3.w_b
  35.6 8.7 %all-to-all-done.1 = bf16[32,16,128]{2,1,0:T(8,128)(2,1)S(1)} async-done(((bf16[32,16,128]{2,1,0:T(8,128)(2,1)}), bf16[32,16,128]{2,1,0:T(8,128)(2,1)S(1)}, u32[]{:S(2)}, u32[]{:S(2)}) %all-to-all-start.1) | async-done | bytes 131104 | tf_op jit(solution)/shard_map/all_to_all | solution.py:253
  44.3 0.3 shard_map.115.p0
  44.6 2.8 %collective-permute-start.6 = (bf16[128,512]{1,0:T(8,128)(2,1)S(1)}, bf16[128,512]{1,0:T(8,128)(2,1)S(1)}, u32[]{:S(2)}, u32[]{:S(2)}) collective-permute-start(bf16[128,512]{1,0:T(8,128)(2,1)S(1)} %shard_map.115.p0), channel_id=1, source_target_pairs={{0,192},{64,128},{128,64},{192,0},{1,193},{65,129},{129,65},{193,1... | collective-permute-start | bytes 393224 | tf_op jit(solution)/shard_map/ppermute | solution.py:303
  47.4 0.3 collective-permute-start.5
  47.8 0.3 collective-permute-start.4
  48.1 0.0 collective-permute-done.7.refs_4_
  48.1 2.8 %collective-permute-done.6.p3 = bf16[128,512]{1,0:T(8,128)(2,1)S(1)} collective-permute-done((bf16[128,512]{1,0:T(8,128)(2,1)S(1)}, bf16[128,512]{1,0:T(8,128)(2,1)S(1)}, u32[]{:S(2)}, u32[]{:S(2)}) %collective-permute-start.6) | collective-permute-done | bytes 131104 | tf_op jit(solution)/shard_map/ppermute | solution.py:303
  50.9 2.0 %collective-permute-done.5.p2 = bf16[128,512]{1,0:T(8,128)(2,1)S(1)} collective-permute-done((bf16[128,512]{1,0:T(8,128)(2,1)S(1)}, bf16[128,512]{1,0:T(8,128)(2,1)S(1)}, u32[]{:S(2)}, u32[]{:S(2)}) %collective-permute-start.5) | collective-permute-done | bytes 131104 | tf_op jit(solution)/shard_map/ppermute | solution.py:303
  52.9 0.0 collective-permute-done.4.p1
  52.9 0.0 copy-done.7
  52.9 0.0 copy-start.1
  52.9 0.9 copy-done.1
  53.8 0.0 copy-start.2
  53.8 0.9 copy-done.2
  54.7 0.0 copy-start.3
  54.7 0.9 copy-done.3
  55.6 0.0 copy-start.4
  55.6 0.9 copy-done.4
  56.5 0.0 copy-start.5
  56.5 0.9 copy-done.5
  57.4 1.3 %shard_map.116 = (bf16[8,16,640]{2,1,0:T(8,128)(2,1)S(1)}, bf16[2,128,256]{2,1,0:T(8,128)(2,1)S(1)}) custom-call(bf16[128,512]{1,0:T(8,128)(2,1)S(1)} %shard_map.115.p0, bf16[128,512]{1,0:T(8,128)(2,1)S(1)} %collective-permute-done.4.p1, bf16[128,512]{1,0:T(8,128)(2,1)S(1)} %collective-permute-done.5.p2, bf16[128,512]{1,0:T(8,128)(2,1)S(1)} %collective-permute-done.6.p3, ...), custom_call_target="tpu_custom_call" | custom-call | flops 100000000 | bytes 1574912 | tf_op jit(solution)/shard_map/pallas_call | solution.py:25
  58.7 11.7 %all_to_all.20.arrived = bf16[8,16,640]{2,1,0:T(8,128)(2,1)S(1)} all-to-all(bf16[8,16,640]{2,1,0:T(8,128)(2,1)S(1)} %get-tuple-element.15), channel_id=1, replica_groups=mesh['y'=4,'x'=4,'z'=8,'c'=2] {'z'}, dimensions={0} | all-to-all | bytes 327680 | tf_op jit(solution)/shard_map/all_to_all | solution.py:253
  70.4 0.7 shard_map.117
  71.2 12.1 %all_to_all.21 = bf16[32,16,128]{2,1,0:T(8,128)(2,1)S(1)} all-to-all(bf16[32,16,128]{2,1,0:T(8,128)(2,1)S(1)} %get-tuple-element.16), channel_id=1, replica_groups=mesh['y'=4,'x'=4,'z'=8,'c'=2] {'x','z'}, dimensions={0} | all-to-all | bytes 262144 | tf_op jit(solution)/shard_map/all_to_all | solution.py:253
  83.3 0.3 shard_map.118.refs_0_
  83.6 3.5 %collective-permute-start.10 = (bf16[128,512]{1,0:T(8,128)(2,1)S(1)}, bf16[128,512]{1,0:T(8,128)(2,1)S(1)}, u32[]{:S(2)}, u32[]{:S(2)}) collective-permute-start(bf16[128,512]{1,0:T(8,128)(2,1)S(1)} %shard_map.118.refs_0_), channel_id=1, source_target_pairs={{0,192},{64,128},{128,64},{192,0},{1,193},{65,129},{129,65},{193,1... | collective-permute-start | bytes 393224 | tf_op jit(solution)/shard_map/ppermute | solution.py:303
  87.1 0.0 collective-permute-start.9
  87.1 0.7 collective-permute-start.8
  87.8 2.6 %collective-permute-done.10.refs_3_ = bf16[128,512]{1,0:T(8,128)(2,1)S(1)} collective-permute-done((bf16[128,512]{1,0:T(8,128)(2,1)S(1)}, bf16[128,512]{1,0:T(8,128)(2,1)S(1)}, u32[]{:S(2)}, u32[]{:S(2)}) %collective-permute-start.10) | collective-permute-done | bytes 131104 | tf_op jit(solution)/shard_map/ppermute | solution.py:303
  90.4 2.0 %collective-permute-done.9.refs_2_ = bf16[128,512]{1,0:T(8,128)(2,1)S(1)} collective-permute-done((bf16[128,512]{1,0:T(8,128)(2,1)S(1)}, bf16[128,512]{1,0:T(8,128)(2,1)S(1)}, u32[]{:S(2)}, u32[]{:S(2)}) %collective-permute-start.9) | collective-permute-done | bytes 131104 | tf_op jit(solution)/shard_map/ppermute | solution.py:303
  92.4 0.0 collective-permute-done.8.refs_1_
  92.4 0.1 shard_map.119
  92.5 5.6 %collective-permute-start.11 = (bf16[128,256]{1,0:T(8,128)(2,1)S(1)}, bf16[128,256]{1,0:T(8,128)(2,1)S(1)}, u32[]{:S(2)}, u32[]{:S(2)}) collective-permute-start(bf16[128,256]{1,0:T(8,128)(2,1)S(1)} %get-tuple-element.19), channel_id=1, source_target_pairs={{0,1},{1,0},{2,3},{3,2},{4,5},{5,4},{6,7},{7,6},{8,9},{9,8},{10,11... | collective-permute-start | bytes 196616 | tf_op jit(solution)/shard_map/ppermute | solution.py:265
  98.1 3.2 %new_states.1 = f32[2,16,1,128,128]{4,3,2,1,0:T(8,128)} custom-call(f32[3,16,128]{2,1,0:T(8,128)S(1)} %get-tuple-element.20.terms_a, f32[3,16,128]{2,1,0:T(8,128)S(1)} %get-tuple-element.21.terms_b, f32[2,16,1,128,128]{4,3,2,1,0:T(8,128)S(1)} %copy-done), custom_call_target="tpu_custom_call" | custom-call | flops 10000000 | bytes 4194304 | tf_op jit(solution)/shard_map/new_states/pallas_call | solution.py:223
  101.2 0.0 collective-permute-done.11.received
  101.2 0.7 shard_map.120
  (1 shorter events, 0.0 us)
Async XLA Ops:
  0.6 24.7 %copy-start.9 = (f32[2,128]{1,0:T(2,128)S(1)}, f32[2,128]{1,0:T(2,128)}, u32[]{:S(2)}) copy-start(f32[2,128]{1,0:T(2,128)} %head_gain.1) | copy-start | bytes 3076
  0.6 24.7 %copy-start.8 = (f32[2,128]{1,0:T(2,128)S(1)}, f32[2,128]{1,0:T(2,128)}, u32[]{:S(2)}) copy-start(f32[2,128]{1,0:T(2,128)} %floor_rate.1) | copy-start | bytes 3076
  0.7 25.5 %copy-start = (f32[2,16,1,128,128]{4,3,2,1,0:T(8,128)S(1)}, f32[2,16,1,128,128]{4,3,2,1,0:T(8,128)}, u32[]{:S(2)}) copy-start(f32[2,16,1,128,128]{4,3,2,1,0:T(8,128)} %state.5) | copy-start | bytes 6291460
  3.2 22.9 %all-to-all-start = ((bf16[16,16,640]{2,1,0:T(8,128)(2,1)}), bf16[16,16,640]{2,1,0:T(8,128)(2,1)S(1)}, u32[]{:S(2)}, u32[]{:S(2)}) async-start(bf16[16,16,640]{2,1,0:T(8,128)(2,1)} %get-tuple-element.12), calls=%async_computation | async-start | bytes 655360 | tf_op jit(solution)/shard_map/all_to_all | solution.py:253
  13.2 6.3 %collective-permute-start = (bf16[2,128,256]{2,1,0:T(8,128)(2,1)}, bf16[2,128,256]{2,1,0:T(8,128)(2,1)S(1)}, u32[]{:S(2)}, u32[]{:S(2)}) collective-permute-start(bf16[2,128,256]{2,1,0:T(8,128)(2,1)} %param.18), channel_id=1, source_target_pairs={{0,16},{16,32},{32,48},{48,0},{1,17},{17,33},{33,49},{49,1},{2,18}... | collective-permute-start | bytes 393224 | tf_op jit(solution)/shard_map/ppermute | solution.py:279
  14.4 5.1 %collective-permute-start.2 = (bf16[2,128,256]{2,1,0:T(8,128)(2,1)}, bf16[2,128,256]{2,1,0:T(8,128)(2,1)S(1)}, u32[]{:S(2)}, u32[]{:S(2)}) collective-permute-start(bf16[2,128,256]{2,1,0:T(8,128)(2,1)} %param.18), channel_id=1, source_target_pairs={{0,48},{16,0},{32,16},{48,32},{1,49},{17,1},{33,17},{49,33},{2,50}... | collective-permute-start | bytes 393224 | tf_op jit(solution)/shard_map/ppermute | solution.py:279
  15.8 7.4 %collective-permute-start.1 = (bf16[2,128,256]{2,1,0:T(8,128)(2,1)}, bf16[2,128,256]{2,1,0:T(8,128)(2,1)S(1)}, u32[]{:S(2)}, u32[]{:S(2)}) collective-permute-start(bf16[2,128,256]{2,1,0:T(8,128)(2,1)} %param.18), channel_id=1, source_target_pairs={{0,32},{16,48},{32,0},{48,16},{1,33},{17,49},{33,1},{49,17},{2,34}... | collective-permute-start | bytes 393224 | tf_op jit(solution)/shard_map/ppermute | solution.py:279
  24.2 28.6 %copy-start.7 = (f32[2,256]{1,0:T(2,128)S(1)}, f32[2,256]{1,0:T(2,128)}, u32[]{:S(2)}) copy-start(f32[2,256]{1,0:T(2,128)} %gain.3) | copy-start | bytes 6148
  24.2 11.3 %collective-permute-start.3 = (bf16[4,2,128,256]{3,2,1,0:T(8,128)(2,1)S(1)}, bf16[4,2,128,256]{3,2,1,0:T(8,128)(2,1)S(1)}, u32[]{:S(2)}, u32[]{:S(2)}) collective-permute-start(bf16[4,2,128,256]{3,2,1,0:T(8,128)(2,1)S(1)} %pad_maximum_fusion.w_a), channel_id=1, source_target_pairs={{0,1},{1,0},{2,3},{3,2},{4,5},{5,4},{6,7},{7,6},{8,9},{9,8},{10,11... | collective-permute-start | bytes 1572872 | tf_op jit(solution)/shard_map/ppermute | solution.py:265
  26.9 0.7 copy-start.6
  27.6 16.8 %all-to-all-start.1 = ((bf16[32,16,128]{2,1,0:T(8,128)(2,1)}), bf16[32,16,128]{2,1,0:T(8,128)(2,1)S(1)}, u32[]{:S(2)}, u32[]{:S(2)}) async-start(bf16[32,16,128]{2,1,0:T(8,128)(2,1)} %copy-done.6), calls=%async_computation.1 | async-start | bytes 262144 | tf_op jit(solution)/shard_map/all_to_all | solution.py:253
  35.2 12.9 %collective-permute-start.7 = (bf16[256,768]{1,0:T(8,128)(2,1)}, bf16[256,768]{1,0:T(8,128)(2,1)}, u32[]{:S(2)}, u32[]{:S(2)}) collective-permute-start(bf16[256,768]{1,0:T(8,128)(2,1)} %get-tuple-element.14), channel_id=1, source_target_pairs={{0,1},{1,0},{2,3},{3,2},{4,5},{5,4},{6,7},{7,6},{8,9},{9,8},{10,11... | collective-permute-start | bytes 1179656 | tf_op jit(solution)/shard_map/ppermute | solution.py:265
  44.6 6.3 %collective-permute-start.6 = (bf16[128,512]{1,0:T(8,128)(2,1)S(1)}, bf16[128,512]{1,0:T(8,128)(2,1)S(1)}, u32[]{:S(2)}, u32[]{:S(2)}) collective-permute-start(bf16[128,512]{1,0:T(8,128)(2,1)S(1)} %shard_map.115.p0), channel_id=1, source_target_pairs={{0,192},{64,128},{128,64},{192,0},{1,193},{65,129},{129,65},{193,1... | collective-permute-start | bytes 393224 | tf_op jit(solution)/shard_map/ppermute | solution.py:303
  47.4 5.4 %collective-permute-start.5 = (bf16[128,512]{1,0:T(8,128)(2,1)S(1)}, bf16[128,512]{1,0:T(8,128)(2,1)S(1)}, u32[]{:S(2)}, u32[]{:S(2)}) collective-permute-start(bf16[128,512]{1,0:T(8,128)(2,1)S(1)} %shard_map.115.p0), channel_id=1, source_target_pairs={{0,128},{64,192},{128,0},{192,64},{1,129},{65,193},{129,1},{193,65... | collective-permute-start | bytes 393224 | tf_op jit(solution)/shard_map/ppermute | solution.py:303
  47.8 5.1 %collective-permute-start.4 = (bf16[128,512]{1,0:T(8,128)(2,1)S(1)}, bf16[128,512]{1,0:T(8,128)(2,1)S(1)}, u32[]{:S(2)}, u32[]{:S(2)}) collective-permute-start(bf16[128,512]{1,0:T(8,128)(2,1)S(1)} %shard_map.115.p0), channel_id=1, source_target_pairs={{0,64},{64,0},{128,192},{192,128},{1,65},{65,1},{129,193},{193,129... | collective-permute-start | bytes 393224 | tf_op jit(solution)/shard_map/ppermute | solution.py:303
  52.9 0.9 copy-start.1
  53.8 0.9 copy-start.2
  54.7 0.9 copy-start.3
  55.6 0.9 copy-start.4
  56.5 0.9 copy-start.5
  83.6 6.8 %collective-permute-start.10 = (bf16[128,512]{1,0:T(8,128)(2,1)S(1)}, bf16[128,512]{1,0:T(8,128)(2,1)S(1)}, u32[]{:S(2)}, u32[]{:S(2)}) collective-permute-start(bf16[128,512]{1,0:T(8,128)(2,1)S(1)} %shard_map.118.refs_0_), channel_id=1, source_target_pairs={{0,192},{64,128},{128,64},{192,0},{1,193},{65,129},{129,65},{193,1... | collective-permute-start | bytes 393224 | tf_op jit(solution)/shard_map/ppermute | solution.py:303
  87.1 5.3 %collective-permute-start.9 = (bf16[128,512]{1,0:T(8,128)(2,1)S(1)}, bf16[128,512]{1,0:T(8,128)(2,1)S(1)}, u32[]{:S(2)}, u32[]{:S(2)}) collective-permute-start(bf16[128,512]{1,0:T(8,128)(2,1)S(1)} %shard_map.118.refs_0_), channel_id=1, source_target_pairs={{0,128},{64,192},{128,0},{192,64},{1,129},{65,193},{129,1},{193,65... | collective-permute-start | bytes 393224 | tf_op jit(solution)/shard_map/ppermute | solution.py:303
  87.1 5.3 %collective-permute-start.8 = (bf16[128,512]{1,0:T(8,128)(2,1)S(1)}, bf16[128,512]{1,0:T(8,128)(2,1)S(1)}, u32[]{:S(2)}, u32[]{:S(2)}) collective-permute-start(bf16[128,512]{1,0:T(8,128)(2,1)S(1)} %shard_map.118.refs_0_), channel_id=1, source_target_pairs={{0,64},{64,0},{128,192},{192,128},{1,65},{65,1},{129,193},{193,129... | collective-permute-start | bytes 393224 | tf_op jit(solution)/shard_map/ppermute | solution.py:303
  92.5 8.7 %collective-permute-start.11 = (bf16[128,256]{1,0:T(8,128)(2,1)S(1)}, bf16[128,256]{1,0:T(8,128)(2,1)S(1)}, u32[]{:S(2)}, u32[]{:S(2)}) collective-permute-start(bf16[128,256]{1,0:T(8,128)(2,1)S(1)} %get-tuple-element.19), channel_id=1, source_target_pairs={{0,1},{1,0},{2,3},{3,2},{4,5},{5,4},{6,7},{7,6},{8,9},{9,8},{10,11... | collective-permute-start | bytes 196616 | tf_op jit(solution)/shard_map/ppermute | solution.py:265

commit v2 on v1

--- a/solution.py
+++ b/solution.py
@@ -61,9 +61,9 @@
         )
 
 
-def start_kernel(tok, gain, *refs):
+def start_kernel(tok, gain, w_output, *refs):
     w = refs[0:4]
-    payload_ref, bundle_ref, tok_here, gain_here, w_here, sems = refs[4:]
+    payload_ref, bundle_ref, out_0, tok_here, gain_here, w_here, o_here, sems = refs[4:]
     core = lax.axis_index("c")
     n_z, _, own_rows, feats = tok.shape
     rows = n_z * own_rows
@@ -71,6 +71,7 @@
         pltpu.make_async_copy(tok, tok_here, sems.at[0]),
         pltpu.make_async_copy(gain, gain_here, sems.at[1]),
         *[pltpu.make_async_copy(w[p], w_here.at[p], sems.at[2 + p]) for p in range(4)],
+        pltpu.make_async_copy(w_output.at[0:1], o_here, sems.at[6]),
     ]
     for copy in copies:
         copy.start()
@@ -79,6 +80,7 @@
     weights = [w_here.at[p] for p in range(4)]
     x = tok_here[...].reshape(2 * rows, feats)
     store(*project(x, gain_here[0:1, :], [v[0] for v in weights]), payload_ref)
+    out_0[...] = o_here[0]
     for p in range(4):
         bundle_ref[:, p * LANES : (p + 1) * LANES] = weights[p][1]
     bundle_ref[0:rows, 4 * LANES :] = tok_here[:, 1 - core].reshape(rows, feats)
@@ -100,14 +102,16 @@
         out_shape=[
             jax.ShapeDtypeStruct((n_dp, own_rows, 5 * LANES), BF16),
             jax.ShapeDtypeStruct((feats, 4 * LANES + feats), BF16),
+            jax.ShapeDtypeStruct(own[2].shape[1:], BF16),
         ],
         in_specs=[hbm] * len(own),
-        out_specs=[vmem] * 2,
+        out_specs=[vmem] * 3,
         scratch_shapes=[
             pltpu.VMEM(own[0].shape, BF16),
             pltpu.VMEM(own[1].shape, F32),
-            pltpu.VMEM((4, *own[2].shape), BF16),
-            pltpu.SemaphoreType.DMA((6,)),
+            pltpu.VMEM((4, *own[3].shape), BF16),
+            pltpu.VMEM((1, *own[2].shape[1:]), BF16),
+            pltpu.SemaphoreType.DMA((7,)),
         ],
         cost_estimate=pl.CostEstimate(flops=10**8, bytes_accessed=10**6, transcendentals=0),
         compiler_params=pltpu.CompilerParams(vmem_limit_bytes=START_LIMIT),
@@ -115,7 +119,7 @@
     )(*own)
 
 
-def rates_kernel(floor_rate, head_gain, out_ref):
+def rates_kernel(floor_rate, head_gain, state, out_ref):
     out_ref[0:2] = floor_rate[...]
     out_ref[2:4] = head_gain[...]
 
@@ -131,7 +135,7 @@
 
 
 def middle_kernel(p0, p1, p2, p3, tok, gain, *refs):
-    w, (bundle, payload_ref, x_ref) = refs[0:4], refs[4:]
+    w, (bundle, payload_ref, keep_ref, send_ref) = refs[0:4], refs[4:]
     core = lax.axis_index("c")
     n_z, _, own_rows, feats = tok.shape
     rows = n_z * own_rows
@@ -144,22 +148,17 @@
     other_w = [bundle[:, p * LANES : (p + 1) * LANES] for p in range(4)]
     others, other_squares = project(halves[1], other_gain, other_w)
     store([t + o for t, o in zip(totals, others)], squares + other_squares, payload_ref)
-    x_ref[0] = halves[0]
-    x_ref[1] = halves[1]
-
-
-def last_kernel(*refs):
-    parts, (x_in, keep_ref, send_ref) = refs[0:4], refs[4:]
-    halves = add_up(parts, [x_in[0], x_in[1]])
     keep_ref[...] = halves[0]
     send_ref[...] = halves[1]
 
 
-def join_kernel(keep, received, out_ref):
+def last_kernel(p0, p1, p2, p3, x_keep, x_other, out_ref):
     core = lax.axis_index("c")
-    n_z, _, own_rows, feats = out_ref.shape
-    out_ref[:, core] = keep[...].reshape(n_z, own_rows, feats)
-    out_ref[:, 1 - core] = received[...].reshape(n_z, own_rows, feats)
+    for parity, x in ((core, x_keep), (1 - core, x_other)):
+        a, b, c, d = [p[:, parity].astype(F32) for p in (p0, p1, p2, p3)]
+        n_z, own_rows, feats = a.shape
+        before = x[...].reshape(n_z, own_rows, feats).astype(F32)
+        out_ref[:, parity] = (before + ((a + b) + (c + d))).astype(BF16)
 
 
 def sigmoid(x):
@@ -232,14 +231,14 @@
     )(terms_a, terms_b, state)
 
 
-def output_kernel(layer, heads, w_a, w_b, out_ref):
+def output_kernel(heads, w_a, w_b, out_ref):
     my_x = lax.axis_index("x")
     n_x = heads.shape[0]
     rows = heads.shape[1] * heads.shape[2]
     for half, w in enumerate((w_a, w_b)):
         total = None
         for i in range(n_x):
-            block = w[lax.rem(my_x - i + n_x, n_x), layer]
+            block = w[lax.rem(my_x - i + n_x, n_x)]
             product = jnp.dot(
                 heads[i].reshape(rows, LANES), block, preferred_element_type=F32
             )
@@ -249,6 +248,20 @@
         out_ref[:, half * feats : (half + 1) * feats] = total
 
 
+def last_output_kernel(heads, other_heads, *refs):
+    pieces, out_ref = refs[:-1], refs[-1]
+    core = lax.axis_index("c")
+    my_x = lax.axis_index("x")
+    n_x, n_z, own_rows, _ = heads.shape
+    for parity, h in ((core, heads), (1 - core, other_heads)):
+        total = None
+        for k in range(n_x):
+            rows = h[lax.rem(my_x - k + n_x, n_x)].reshape(n_z * own_rows, LANES)
+            product = jnp.dot(rows, pieces[k][1], preferred_element_type=F32)
+            total = product if total is None else total + product
+        out_ref[:, parity] = total.astype(BF16).reshape(n_z, own_rows, total.shape[1])
+
+
 def spread(copies, axes):
     return lax.all_to_all(copies, axes, split_axis=0, concat_axis=0, tiled=True)
 
@@ -267,18 +280,22 @@
     weights = (w_query, w_forget, w_value, w_gate)
     tok = tokens.reshape(n_z, 2, own_rows, feats)
     payload_shape = jax.ShapeDtypeStruct((n_z, own_rows, 5 * LANES), BF16)
-    x_shape = jax.ShapeDtypeStruct((2, rows, feats), BF16)
-    payload, bundle = start(2 * n_z, own_rows, tok, norm_gain, *weights)
+    payload, bundle, w_out_0 = start(2 * n_z, own_rows, tok, norm_gain, w_output, *weights)
     (rates,) = call(
         rates_kernel, [jax.ShapeDtypeStruct((8, LANES), F32)],
-        floor_rate, head_gain, flops=10**4,
+        floor_rate, head_gain, state, flops=10**4,
     )
     bundle_b = swap(bundle)
-    pieces = [w_output]
-    for k in range(1, n_x):
-        pieces.append(lax.ppermute(w_output, "x", [(i, (i + k) % n_x) for i in range(n_x)]))
+
+    def gather(w):
+        return [
+            lax.ppermute(w, "x", [(i, (i + k) % n_x) for i in range(n_x)]) for k in range(1, n_x)
+        ]
+
+    pieces = [w_out_0, *gather(w_out_0)]
     gathered = jnp.stack(pieces)
     w_out = (gathered, swap(gathered))
+    late = [w_output, *gather(w_output)]
 
     terms = []
     for layer in range(2):
@@ -293,27 +310,29 @@
         )
         terms.append(term)
         heads = spread(gated, ("x", "z")).reshape(n_x, n_z, own_rows, LANES)
-        (own,) = call(
-            functools.partial(output_kernel, layer),
-            [jax.ShapeDtypeStruct((rows, 2 * feats), BF16)],
-            heads, *w_out, flops=10**8,
-        )
+        if layer == 0:
+            shape = jax.ShapeDtypeStruct((rows, 2 * feats), BF16)
+            operands = (output_kernel, [shape], heads, *w_out)
+        else:
+            other_heads = swap(heads)
+            shape = jax.ShapeDtypeStruct((n_z, 2, own_rows, feats), BF16)
+            operands = (last_output_kernel, [shape], heads, other_heads, *late)
+        (own,) = call(*operands, flops=10**8)
         parts = [own]
         for k in range(1, n_y):
             parts.append(lax.ppermute(own, "y", [(i, i ^ k) for i in range(n_y)]))
         if layer == 0:
-            payload, x = call(
-                middle_kernel, [payload_shape, x_shape],
+            half = jax.ShapeDtypeStruct((rows, feats), BF16)
+            payload, x_keep, x_send = call(
+                middle_kernel, [payload_shape, half, half],
                 *parts, tok, norm_gain, *weights, bundle_b, flops=10**8,
             )
-    half = jax.ShapeDtypeStruct((rows, feats), BF16)
-    keep, send = call(last_kernel, [half, half], *parts, x, flops=10**6)
+    x_other = swap(x_send)
+    (mixed,) = call(
+        last_kernel, [jax.ShapeDtypeStruct((n_z, 2, own_rows, feats), BF16)],
+        *parts, x_keep, x_other, flops=10**6,
+    )
     states = new_states(*terms, state)
-    received = swap(send)
-    (mixed,) = call(
-        join_kernel, [jax.ShapeDtypeStruct((n_z, 2, own_rows, feats), BF16)],
-        keep, received, flops=10**6,
-    )
     return mixed.reshape(batch, feats), states
 
 

time: 102 us -> 101 us (level)
  blocking collectives: 23.8 us -> 11.8 us
  starting transfers between devices: 36.6 us -> 45.3 us
  Pallas kernels: 9.83 us -> 12 us
    all_to_all x2 -> x1, blocking collectives: 23.8 us -> 11.8 us  [spread(): return lax.all_to_all(copies, axes, split_axis=0, concat_axis=0, tiled=True)]
    ppermute x3 -> x6, starting transfers between devices: 4.21 us -> 9.09 us  [gather(): lax.ppermute(w, 'x', [(i, (i + k) % n_x) for i in range(n_x)])]
    all_to_all x2 -> x3, starting transfers between devices: 17.6 us -> 21.3 us  [spread(): return lax.all_to_all(copies, axes, split_axis=0, concat_axis=0, tiled=True)]
    ppermute x6, waiting for transfers between devices: 9.39 us -> 6.21 us  [per_device(): parts.append(lax.ppermute(own, 'y', [(i, i ^ k) for i in range(n_y)]))]
    all_to_all x2 -> x3, waiting for transfers between devices: 9.5 us -> 12.4 us  [spread(): return lax.all_to_all(copies, axes, split_axis=0, concat_axis=0, tiled=True)]
    pallas_call x8 -> x7, Pallas kernels: 4.14 us -> 6.39 us  [call(): pl.pallas_call(kernel, out_shape=outs, in_specs=[vmem] * len(args), out_s...]
    ppermute x3 -> x4, starting transfers between devices: 7.1 us -> 8.15 us  [swap(): return lax.ppermute(v, 'c', [(0, 1), (1, 0)])]
    unnamed x20 -> x22, local copies, waits for them, and re-layouts: 5.19 us -> 4.51 us
  transfers between devices with their start and end apart: 14 -> 19, of which waited for: 8 -> 10; matrix products, arithmetic and copies ran while one was open for 1% -> 1% of each run, Pallas kernels for 4% -> 6%
where the time goes in v2:
time: 101 us
  starting transfers between devices  45.3 us (45%)
  waiting for transfers between devices  25.3 us (25%)
  Pallas kernels  12 us (12%)
  blocking collectives  11.8 us (12%)
  local copies, waits for them, and re-layouts  4.51 us (4%)
    all_to_all x3, starting transfers between devices, spread(): return lax.all_to_all(copies, axes, split_axis=0, concat_axis=0, tiled=True)  21.3 us
    all_to_all x3, waiting for transfers between devices, spread(): return lax.all_to_all(copies, axes, split_axis=0, concat_axis=0, tiled=True)  12.4 us
    all_to_all x1, blocking collectives, spread(): return lax.all_to_all(copies, axes, split_axis=0, concat_axis=0, tiled=True)  11.8 us
    ppermute x6, starting transfers between devices, gather(): lax.ppermute(w, 'x', [(i, (i + k) % n_x) for i in range(n_x)])  9.09 us
    ppermute x4, starting transfers between devices, swap(): return lax.ppermute(v, 'c', [(0, 1), (1, 0)])  8.15 us
    ppermute x6, starting transfers between devices, per_device(): parts.append(lax.ppermute(own, 'y', [(i, i ^ k) for i in range(n_y)]))  6.84 us
    pallas_call x7, Pallas kernels, call(): pl.pallas_call(kernel, out_shape=outs, in_specs=[vmem] * len(args), out_s...  6.39 us
    ppermute x6, waiting for transfers between devices, per_device(): parts.append(lax.ppermute(own, 'y', [(i, i ^ k) for i in range(n_y)]))  6.21 us
  transfers between devices with their start and end apart: 19, of which 10 were waited for; matrix products, arithmetic and copies ran while one was open for 1% of the time, Pallas kernels for 6%

profile of v2, /device:TPU:1, one launch (start us, length us, event | category | flops | bytes accessed | tf_op | source)
XLA Modules:
  0.0 100.5 jit_solution(10504618669423693437)
XLA Ops:
  0.6 2.4 %start.1 = (bf16[16,16,640]{2,1,0:T(8,128)(2,1)}, bf16[256,768]{1,0:T(8,128)(2,1)}, bf16[128,256]{1,0:T(8,128)(2,1)}) custom-call(bf16[8,2,16,256]{3,2,1,0:T(8,128)(2,1)} %bitcast.10, f32[2,256]{1,0:T(2,128)} %gain.3, bf16[2,128,256]{2,1,0:T(8,128)(2,1)} %refs_0_.5, bf16[2,256,128]{2,1,0:T(8,128)(2,1)} %refs_0_.4, bf16[2,256,128]{2,1,0:T(8,128)(2,1)} %refs_1_.3, ...), custom_call_target="tpu_custom_call" | custom-call | flops 100000000 | bytes 1000000 | tf_op jit(solution)/shard_map/start/pallas_call | solution.py:100
  3.0 10.0 %all-to-all-start = ((bf16[16,16,640]{2,1,0:T(8,128)(2,1)}), bf16[16,16,640]{2,1,0:T(8,128)(2,1)S(1)}, u32[]{:S(2)}, u32[]{:S(2)}) async-start(bf16[16,16,640]{2,1,0:T(8,128)(2,1)} %get-tuple-element.12), calls=%async_computation | async-start | bytes 655360 | tf_op jit(solution)/shard_map/all_to_all | solution.py:266
  13.0 2.5 %collective-permute-start.2 = (bf16[128,256]{1,0:T(8,128)(2,1)}, bf16[128,256]{1,0:T(8,128)(2,1)S(1)}, u32[]{:S(2)}, u32[]{:S(2)}) collective-permute-start(bf16[128,256]{1,0:T(8,128)(2,1)} %get-tuple-element.14), channel_id=1, source_target_pairs={{0,48},{16,0},{32,16},{48,32},{1,49},{17,1},{33,17},{49,33},{2,50}... | collective-permute-start | bytes 196616 | tf_op jit(solution)/shard_map/ppermute | solution.py:292
  15.5 0.5 collective-permute-start.1
  16.0 0.6 collective-permute-start
  16.6 0.5 collective-permute-done.2
  17.2 3.5 %collective-permute-done.1 = bf16[128,256]{1,0:T(8,128)(2,1)S(1)} collective-permute-done((bf16[128,256]{1,0:T(8,128)(2,1)}, bf16[128,256]{1,0:T(8,128)(2,1)S(1)}, u32[]{:S(2)}, u32[]{:S(2)}) %collective-permute-start.1) | collective-permute-done | bytes 65568 | tf_op jit(solution)/shard_map/ppermute | solution.py:292
  20.6 1.6 %collective-permute-done = bf16[128,256]{1,0:T(8,128)(2,1)S(1)} collective-permute-done((bf16[128,256]{1,0:T(8,128)(2,1)}, bf16[128,256]{1,0:T(8,128)(2,1)S(1)}, u32[]{:S(2)}, u32[]{:S(2)}) %collective-permute-start) | collective-permute-done | bytes 65568 | tf_op jit(solution)/shard_map/ppermute | solution.py:292
  22.3 0.9 pad_maximum_fusion.w_a
  23.2 1.0 collective-permute-start.3
  24.1 1.6 %copy-done = f32[2,16,1,128,128]{4,3,2,1,0:T(8,128)S(1)} copy-done((f32[2,16,1,128,128]{4,3,2,1,0:T(8,128)S(1)}, f32[2,16,1,128,128]{4,3,2,1,0:T(8,128)}, u32[]{:S(2)}) %copy-start) | copy-done | bytes 2097176
  25.7 0.7 copy-done.9
  26.4 0.7 copy-done.10
  27.1 0.0 copy-start.4
  27.1 0.0 copy-start.5
  27.1 0.0 copy-start.6
  27.1 0.0 copy-start.8
  27.1 0.0 all-to-all-done.arrived
  27.1 1.5 %copy-done.1 = f32[2,16,1,128,128]{4,3,2,1,0:T(8,128)S(1)} copy-done((f32[2,16,1,128,128]{4,3,2,1,0:T(8,128)S(1)}, f32[2,16,1,128,128]{4,3,2,1,0:T(8,128)}, u32[]{:S(2)}) %copy-start.1) | copy-done | bytes 2097176
  28.6 1.4 %shard_map.114 = (bf16[32,16,128]{2,1,0:T(8,128)(2,1)}, f32[3,16,128]{2,1,0:T(8,128)S(1)}) custom-call(bf16[16,16,640]{2,1,0:T(8,128)(2,1)S(1)} %all-to-all-done.arrived, f32[8,128]{1,0:T(8,128)S(1)} %shard_map.113.rates, f32[2,16,1,128,128]{4,3,2,1,0:T(8,128)S(1)} %copy-done.1), custom_call_target="tpu_custom_call" | custom-call | flops 10000000 | bytes 2428928 | tf_op jit(solution)/shard_map/pallas_call | solution.py:25
  30.1 7.4 %all-to-all-start.1 = ((bf16[32,16,128]{2,1,0:T(8,128)(2,1)}), bf16[32,16,128]{2,1,0:T(8,128)(2,1)S(1)}, u32[]{:S(2)}, u32[]{:S(2)}) async-start(bf16[32,16,128]{2,1,0:T(8,128)(2,1)} %get-tuple-element.13), calls=%async_computation.1 | async-start | bytes 262144 | tf_op jit(solution)/shard_map/all_to_all | solution.py:266
  37.5 0.4 collective-permute-start.7
  37.9 0.0 collective-permute-done.3.w_b
  37.9 8.8 %all-to-all-done.1 = bf16[32,16,128]{2,1,0:T(8,128)(2,1)S(1)} async-done(((bf16[32,16,128]{2,1,0:T(8,128)(2,1)}), bf16[32,16,128]{2,1,0:T(8,128)(2,1)S(1)}, u32[]{:S(2)}, u32[]{:S(2)}) %all-to-all-start.1) | async-done | bytes 131104 | tf_op jit(solution)/shard_map/all_to_all | solution.py:266
  46.6 1.2 %shard_map.115.p0 = bf16[128,512]{1,0:T(8,128)(2,1)S(1)} custom-call(bf16[4,8,16,128]{3,2,1,0:T(8,128)(2,1)S(1)} %bitcast.12, bf16[4,128,256]{2,1,0:T(8,128)(2,1)S(1)} %pad_maximum_fusion.w_a, bf16[4,128,256]{2,1,0:T(8,128)(2,1)} %collective-permute-done.3.w_b), custom_call_target="tpu_custom_call" | custom-call | flops 100000000 | bytes 655360 | tf_op jit(solution)/shard_map/pallas_call | solution.py:25
  47.9 0.0 copy-start.7
  47.9 2.8 %collective-permute-start.6 = (bf16[128,512]{1,0:T(8,128)(2,1)S(1)}, bf16[128,512]{1,0:T(8,128)(2,1)S(1)}, u32[]{:S(2)}, u32[]{:S(2)}) collective-permute-start(bf16[128,512]{1,0:T(8,128)(2,1)S(1)} %shard_map.115.p0), channel_id=1, source_target_pairs={{0,192},{64,128},{128,64},{192,0},{1,193},{65,129},{129,65},{193,1... | collective-permute-start | bytes 393224 | tf_op jit(solution)/shard_map/ppermute | solution.py:323
  50.7 0.4 collective-permute-start.5
  51.1 0.3 collective-permute-start.4
  51.4 0.0 collective-permute-done.7.refs_4_
  51.4 2.8 %collective-permute-done.6.p3 = bf16[128,512]{1,0:T(8,128)(2,1)S(1)} collective-permute-done((bf16[128,512]{1,0:T(8,128)(2,1)S(1)}, bf16[128,512]{1,0:T(8,128)(2,1)S(1)}, u32[]{:S(2)}, u32[]{:S(2)}) %collective-permute-start.6) | collective-permute-done | bytes 131104 | tf_op jit(solution)/shard_map/ppermute | solution.py:323
  54.2 2.0 %collective-permute-done.5.p2 = bf16[128,512]{1,0:T(8,128)(2,1)S(1)} collective-permute-done((bf16[128,512]{1,0:T(8,128)(2,1)S(1)}, bf16[128,512]{1,0:T(8,128)(2,1)S(1)}, u32[]{:S(2)}, u32[]{:S(2)}) %collective-permute-start.5) | collective-permute-done | bytes 131104 | tf_op jit(solution)/shard_map/ppermute | solution.py:323
  56.1 0.0 collective-permute-done.4.p1
  56.1 0.0 copy-done.2
  56.1 0.0 copy-done.3
  56.1 0.0 copy-done.4
  56.2 0.0 copy-done.5
  56.2 0.0 copy-done.6
  56.2 0.0 copy-done.8
  56.2 1.3 %shard_map.116 = (bf16[8,16,640]{2,1,0:T(8,128)(2,1)S(1)}, bf16[128,256]{1,0:T(8,128)(2,1)S(1)}, bf16[128,256]{1,0:T(8,128)(2,1)S(1)}) custom-call(bf16[128,512]{1,0:T(8,128)(2,1)S(1)} %shard_map.115.p0, bf16[128,512]{1,0:T(8,128)(2,1)S(1)} %collective-permute-done.4.p1, bf16[128,512]{1,0:T(8,128)(2,1)S(1)} %collective-permute-done.5.p2, ...), custom_call_target="tpu_custom_call" | custom-call | flops 100000000 | bytes 1574912 | tf_op jit(solution)/shard_map/pallas_call | solution.py:25
  57.5 11.8 %all_to_all.20.arrived = bf16[8,16,640]{2,1,0:T(8,128)(2,1)S(1)} all-to-all(bf16[8,16,640]{2,1,0:T(8,128)(2,1)S(1)} %get-tuple-element.16), channel_id=1, replica_groups=mesh['y'=4,'x'=4,'z'=8,'c'=2] {'z'}, dimensions={0} | all-to-all | bytes 327680 | tf_op jit(solution)/shard_map/all_to_all | solution.py:266
  69.3 1.4 %shard_map.117 = (bf16[32,16,128]{2,1,0:T(8,128)(2,1)}, f32[3,16,128]{2,1,0:T(8,128)S(1)}) custom-call(bf16[8,16,640]{2,1,0:T(8,128)(2,1)S(1)} %all_to_all.20.arrived, f32[8,128]{1,0:T(8,128)S(1)} %shard_map.113.rates, f32[2,16,1,128,128]{4,3,2,1,0:T(8,128)S(1)} %copy-done.1), custom_call_target="tpu_custom_call" | custom-call | flops 10000000 | bytes 2265088 | tf_op jit(solution)/shard_map/pallas_call | solution.py:25
  70.7 3.9 %all-to-all-start.3 = ((bf16[32,16,128]{2,1,0:T(8,128)(2,1)}), bf16[32,16,128]{2,1,0:T(8,128)(2,1)S(1)}, u32[]{:S(2)}, u32[]{:S(2)}) async-start(bf16[32,16,128]{2,1,0:T(8,128)(2,1)} %get-tuple-element.17), calls=%async_computation.3 | async-start | bytes 262144 | tf_op jit(solution)/shard_map/all_to_all | solution.py:266
  74.6 0.0 copy-done.7
  74.6 2.8 %collective-permute-start.10 = (bf16[2,128,256]{2,1,0:T(8,128)(2,1)S(1)}, bf16[2,128,256]{2,1,0:T(8,128)(2,1)S(1)}, u32[]{:S(2)}, u32[]{:S(2)}) collective-permute-start(bf16[2,128,256]{2,1,0:T(8,128)(2,1)S(1)} %copy-done.7), channel_id=1, source_target_pairs={{0,32},{16,48},{32,0},{48,16},{1,33},{17,49},{33,1},{49,17},{2,34}... | collective-permute-start | bytes 393224 | tf_op jit(solution)/shard_map/ppermute | solution.py:292
  77.4 0.3 collective-permute-start.9
  77.7 2.3 %collective-permute-start.11 = (bf16[2,128,256]{2,1,0:T(8,128)(2,1)S(1)}, bf16[2,128,256]{2,1,0:T(8,128)(2,1)S(1)}, u32[]{:S(2)}, u32[]{:S(2)}) collective-permute-start(bf16[2,128,256]{2,1,0:T(8,128)(2,1)S(1)} %copy-done.7), channel_id=1, source_target_pairs={{0,48},{16,0},{32,16},{48,32},{1,49},{17,1},{33,17},{49,33},{2,50}... | collective-permute-start | bytes 393224 | tf_op jit(solution)/shard_map/ppermute | solution.py:292
  80.1 3.7 %all-to-all-done.3 = bf16[32,16,128]{2,1,0:T(8,128)(2,1)S(1)} async-done(((bf16[32,16,128]{2,1,0:T(8,128)(2,1)}), bf16[32,16,128]{2,1,0:T(8,128)(2,1)S(1)}, u32[]{:S(2)}, u32[]{:S(2)}) %all-to-all-start.3) | async-done | bytes 131104 | tf_op jit(solution)/shard_map/all_to_all | solution.py:266
  83.7 5.6 %collective-permute-start.8 = (bf16[4,8,16,128]{3,2,1,0:T(8,128)(2,1)S(1)}, bf16[4,8,16,128]{3,2,1,0:T(8,128)(2,1)S(1)}, u32[]{:S(2)}, u32[]{:S(2)}) collective-permute-start(bf16[4,8,16,128]{3,2,1,0:T(8,128)(2,1)S(1)} %bitcast.8), channel_id=1, source_target_pairs={{0,1},{1,0},{2,3},{3,2},{4,5},{5,4},{6,7},{7,6},{8,9},{9,8},{10,11... | collective-permute-start | bytes 393224 | tf_op jit(solution)/shard_map/ppermute | solution.py:278
  89.3 0.0 collective-permute-done.10.refs_2_
  89.3 0.0 collective-permute-done.9.refs_1_
  89.3 0.0 collective-permute-done.11.refs_3_
  89.3 1.0 collective-permute-done.8.other_heads
  90.3 0.3 shard_map.118.p0
  90.6 1.9 %collective-permute-start.14 = (bf16[8,2,16,256]{3,2,1,0:T(8,128)(2,1)S(1)}, bf16[8,2,16,256]{3,2,1,0:T(8,128)(2,1)S(1)}, u32[]{:S(2)}, u32[]{:S(2)}) collective-permute-start(bf16[8,2,16,256]{3,2,1,0:T(8,128)(2,1)S(1)} %shard_map.118.p0), channel_id=1, source_target_pairs={{0,192},{64,128},{128,64},{192,0},{1,193},{65,129},{129,65},{193,1... | collective-permute-start | bytes 393224 | tf_op jit(solution)/shard_map/ppermute | solution.py:323
  92.5 0.3 collective-permute-start.13
  92.8 1.2 %collective-permute-start.12 = (bf16[8,2,16,256]{3,2,1,0:T(8,128)(2,1)S(1)}, bf16[8,2,16,256]{3,2,1,0:T(8,128)(2,1)S(1)}, u32[]{:S(2)}, u32[]{:S(2)}) collective-permute-start(bf16[8,2,16,256]{3,2,1,0:T(8,128)(2,1)S(1)} %shard_map.118.p0), channel_id=1, source_target_pairs={{0,64},{64,0},{128,192},{192,128},{1,65},{65,1},{129,193},{193,129... | collective-permute-start | bytes 393224 | tf_op jit(solution)/shard_map/ppermute | solution.py:323
  93.9 1.2 %collective-permute-start.15 = (bf16[128,256]{1,0:T(8,128)(2,1)S(1)}, bf16[128,256]{1,0:T(8,128)(2,1)S(1)}, u32[]{:S(2)}, u32[]{:S(2)}) collective-permute-start(bf16[128,256]{1,0:T(8,128)(2,1)S(1)} %get-tuple-element.19), channel_id=1, source_target_pairs={{0,1},{1,0},{2,3},{3,2},{4,5},{5,4},{6,7},{7,6},{8,9},{9,8},{10,11... | collective-permute-start | bytes 196616 | tf_op jit(solution)/shard_map/ppermute | solution.py:278
  95.1 3.2 %new_states.1 = f32[2,16,1,128,128]{4,3,2,1,0:T(8,128)} custom-call(f32[3,16,128]{2,1,0:T(8,128)S(1)} %get-tuple-element.20.terms_a, f32[3,16,128]{2,1,0:T(8,128)S(1)} %get-tuple-element.21.terms_b, f32[2,16,1,128,128]{4,3,2,1,0:T(8,128)S(1)} %copy-done.1), custom_call_target="tpu_custom_call" | custom-call | flops 10000000 | bytes 4194304 | tf_op jit(solution)/shard_map/new_states/pallas_call | solution.py:222
  98.3 0.0 collective-permute-done.15.x_other
  98.3 0.0 collective-permute-done.14.p3
  98.3 0.2 collective-permute-done.13.p2
  98.5 1.3 %collective-permute-done.12.p1 = bf16[8,2,16,256]{3,2,1,0:T(8,128)(2,1)S(1)} collective-permute-done((bf16[8,2,16,256]{3,2,1,0:T(8,128)(2,1)S(1)}, bf16[8,2,16,256]{3,2,1,0:T(8,128)(2,1)S(1)}, u32[]{:S(2)}, u32[]{:S(2)}) %collective-permute-start.12) | collective-permute-done | bytes 131104 | tf_op jit(solution)/shard_map/ppermute | solution.py:323
  99.8 0.7 shard_map.119
  (7 shorter events, 0.0 us)
Async XLA Ops:
  3.0 24.1 %all-to-all-start = ((bf16[16,16,640]{2,1,0:T(8,128)(2,1)}), bf16[16,16,640]{2,1,0:T(8,128)(2,1)S(1)}, u32[]{:S(2)}, u32[]{:S(2)}) async-start(bf16[16,16,640]{2,1,0:T(8,128)(2,1)} %get-tuple-element.12), calls=%async_computation | async-start | bytes 655360 | tf_op jit(solution)/shard_map/all_to_all | solution.py:266
  13.0 4.1 %collective-permute-start.2 = (bf16[128,256]{1,0:T(8,128)(2,1)}, bf16[128,256]{1,0:T(8,128)(2,1)S(1)}, u32[]{:S(2)}, u32[]{:S(2)}) collective-permute-start(bf16[128,256]{1,0:T(8,128)(2,1)} %get-tuple-element.14), channel_id=1, source_target_pairs={{0,48},{16,0},{32,16},{48,32},{1,49},{17,1},{33,17},{49,33},{2,50}... | collective-permute-start | bytes 196616 | tf_op jit(solution)/shard_map/ppermute | solution.py:292
  15.5 5.1 %collective-permute-start.1 = (bf16[128,256]{1,0:T(8,128)(2,1)}, bf16[128,256]{1,0:T(8,128)(2,1)S(1)}, u32[]{:S(2)}, u32[]{:S(2)}) collective-permute-start(bf16[128,256]{1,0:T(8,128)(2,1)} %get-tuple-element.14), channel_id=1, source_target_pairs={{0,32},{16,48},{32,0},{48,16},{1,33},{17,49},{33,1},{49,17},{2,34}... | collective-permute-start | bytes 196616 | tf_op jit(solution)/shard_map/ppermute | solution.py:292
  16.0 6.2 %collective-permute-start = (bf16[128,256]{1,0:T(8,128)(2,1)}, bf16[128,256]{1,0:T(8,128)(2,1)S(1)}, u32[]{:S(2)}, u32[]{:S(2)}) collective-permute-start(bf16[128,256]{1,0:T(8,128)(2,1)} %get-tuple-element.14), channel_id=1, source_target_pairs={{0,16},{16,32},{32,48},{48,0},{1,17},{17,33},{33,49},{49,1},{2,18}... | collective-permute-start | bytes 196616 | tf_op jit(solution)/shard_map/ppermute | solution.py:292
  23.2 14.7 %collective-permute-start.3 = (bf16[4,128,256]{2,1,0:T(8,128)(2,1)S(1)}, bf16[4,128,256]{2,1,0:T(8,128)(2,1)}, u32[]{:S(2)}, u32[]{:S(2)}) collective-permute-start(bf16[4,128,256]{2,1,0:T(8,128)(2,1)S(1)} %pad_maximum_fusion.w_a), channel_id=1, source_target_pairs={{0,1},{1,0},{2,3},{3,2},{4,5},{5,4},{6,7},{7,6},{8,9},{9,8},{10,11... | collective-permute-start | bytes 786440 | tf_op jit(solution)/shard_map/ppermute | solution.py:278
  24.1 1.6 %copy-start = (f32[2,16,1,128,128]{4,3,2,1,0:T(8,128)S(1)}, f32[2,16,1,128,128]{4,3,2,1,0:T(8,128)}, u32[]{:S(2)}) copy-start(f32[2,16,1,128,128]{4,3,2,1,0:T(8,128)} %state.7) | copy-start | bytes 6291460
  25.7 0.7 copy-start.9
  26.4 0.7 copy-start.10
  27.1 1.6 %copy-start.1 = (f32[2,16,1,128,128]{4,3,2,1,0:T(8,128)S(1)}, f32[2,16,1,128,128]{4,3,2,1,0:T(8,128)}, u32[]{:S(2)}) copy-start(f32[2,16,1,128,128]{4,3,2,1,0:T(8,128)} %state.7) | copy-start | bytes 6291460
  27.1 29.1 %copy-start.2 = (bf16[256,256]{1,0:T(8,128)(2,1)S(1)}, bf16[256,256]{1,0:T(8,128)(2,1)}, u32[]{:S(2)}) copy-start(bf16[256,256]{1,0:T(8,128)(2,1)} %param.10) | copy-start | bytes 393220
  27.1 29.1 %copy-start.3 = (bf16[2,256,128]{2,1,0:T(8,128)(2,1)S(1)}, bf16[2,256,128]{2,1,0:T(8,128)(2,1)}, u32[]{:S(2)}) copy-start(bf16[2,256,128]{2,1,0:T(8,128)(2,1)} %refs_0_.4) | copy-start | bytes 393220
  27.1 29.1 %copy-start.4 = (bf16[2,256,128]{2,1,0:T(8,128)(2,1)S(1)}, bf16[2,256,128]{2,1,0:T(8,128)(2,1)}, u32[]{:S(2)}) copy-start(bf16[2,256,128]{2,1,0:T(8,128)(2,1)} %refs_1_.3) | copy-start | bytes 393220
  27.1 29.1 %copy-start.5 = (bf16[2,256,128]{2,1,0:T(8,128)(2,1)S(1)}, bf16[2,256,128]{2,1,0:T(8,128)(2,1)}, u32[]{:S(2)}) copy-start(bf16[2,256,128]{2,1,0:T(8,128)(2,1)} %refs_2_.3) | copy-start | bytes 393220
  27.1 29.1 %copy-start.6 = (bf16[2,256,128]{2,1,0:T(8,128)(2,1)S(1)}, bf16[2,256,128]{2,1,0:T(8,128)(2,1)}, u32[]{:S(2)}) copy-start(bf16[2,256,128]{2,1,0:T(8,128)(2,1)} %refs_3_.3) | copy-start | bytes 393220
  27.1 29.1 %copy-start.8 = (f32[2,256]{1,0:T(2,128)S(1)}, f32[2,256]{1,0:T(2,128)}, u32[]{:S(2)}) copy-start(f32[2,256]{1,0:T(2,128)} %gain.3) | copy-start | bytes 6148
  30.1 16.6 %all-to-all-start.1 = ((bf16[32,16,128]{2,1,0:T(8,128)(2,1)}), bf16[32,16,128]{2,1,0:T(8,128)(2,1)S(1)}, u32[]{:S(2)}, u32[]{:S(2)}) async-start(bf16[32,16,128]{2,1,0:T(8,128)(2,1)} %get-tuple-element.13), calls=%async_computation.1 | async-start | bytes 262144 | tf_op jit(solution)/shard_map/all_to_all | solution.py:266
  37.5 13.9 %collective-permute-start.7 = (bf16[256,768]{1,0:T(8,128)(2,1)}, bf16[256,768]{1,0:T(8,128)(2,1)}, u32[]{:S(2)}, u32[]{:S(2)}) collective-permute-start(bf16[256,768]{1,0:T(8,128)(2,1)} %get-tuple-element.15), channel_id=1, source_target_pairs={{0,1},{1,0},{2,3},{3,2},{4,5},{5,4},{6,7},{7,6},{8,9},{9,8},{10,11... | collective-permute-start | bytes 1179656 | tf_op jit(solution)/shard_map/ppermute | solution.py:278
  47.9 26.7 %copy-start.7 = (bf16[2,128,256]{2,1,0:T(8,128)(2,1)S(1)}, bf16[2,128,256]{2,1,0:T(8,128)(2,1)}, u32[]{:S(2)}) copy-start(bf16[2,128,256]{2,1,0:T(8,128)(2,1)} %refs_0_.5) | copy-start | bytes 393220
  47.9 6.3 %collective-permute-start.6 = (bf16[128,512]{1,0:T(8,128)(2,1)S(1)}, bf16[128,512]{1,0:T(8,128)(2,1)S(1)}, u32[]{:S(2)}, u32[]{:S(2)}) collective-permute-start(bf16[128,512]{1,0:T(8,128)(2,1)S(1)} %shard_map.115.p0), channel_id=1, source_target_pairs={{0,192},{64,128},{128,64},{192,0},{1,193},{65,129},{129,65},{193,1... | collective-permute-start | bytes 393224 | tf_op jit(solution)/shard_map/ppermute | solution.py:323
  50.7 5.4 %collective-permute-start.5 = (bf16[128,512]{1,0:T(8,128)(2,1)S(1)}, bf16[128,512]{1,0:T(8,128)(2,1)S(1)}, u32[]{:S(2)}, u32[]{:S(2)}) collective-permute-start(bf16[128,512]{1,0:T(8,128)(2,1)S(1)} %shard_map.115.p0), channel_id=1, source_target_pairs={{0,128},{64,192},{128,0},{192,64},{1,129},{65,193},{129,1},{193,65... | collective-permute-start | bytes 393224 | tf_op jit(solution)/shard_map/ppermute | solution.py:323
  51.1 5.1 %collective-permute-start.4 = (bf16[128,512]{1,0:T(8,128)(2,1)S(1)}, bf16[128,512]{1,0:T(8,128)(2,1)S(1)}, u32[]{:S(2)}, u32[]{:S(2)}) collective-permute-start(bf16[128,512]{1,0:T(8,128)(2,1)S(1)} %shard_map.115.p0), channel_id=1, source_target_pairs={{0,64},{64,0},{128,192},{192,128},{1,65},{65,1},{129,193},{193,129... | collective-permute-start | bytes 393224 | tf_op jit(solution)/shard_map/ppermute | solution.py:323
  70.7 13.0 %all-to-all-start.3 = ((bf16[32,16,128]{2,1,0:T(8,128)(2,1)}), bf16[32,16,128]{2,1,0:T(8,128)(2,1)S(1)}, u32[]{:S(2)}, u32[]{:S(2)}) async-start(bf16[32,16,128]{2,1,0:T(8,128)(2,1)} %get-tuple-element.17), calls=%async_computation.3 | async-start | bytes 262144 | tf_op jit(solution)/shard_map/all_to_all | solution.py:266
  74.6 14.8 %collective-permute-start.10 = (bf16[2,128,256]{2,1,0:T(8,128)(2,1)S(1)}, bf16[2,128,256]{2,1,0:T(8,128)(2,1)S(1)}, u32[]{:S(2)}, u32[]{:S(2)}) collective-permute-start(bf16[2,128,256]{2,1,0:T(8,128)(2,1)S(1)} %copy-done.7), channel_id=1, source_target_pairs={{0,32},{16,48},{32,0},{48,16},{1,33},{17,49},{33,1},{49,17},{2,34}... | collective-permute-start | bytes 393224 | tf_op jit(solution)/shard_map/ppermute | solution.py:292
  77.4 12.0 %collective-permute-start.9 = (bf16[2,128,256]{2,1,0:T(8,128)(2,1)S(1)}, bf16[2,128,256]{2,1,0:T(8,128)(2,1)S(1)}, u32[]{:S(2)}, u32[]{:S(2)}) collective-permute-start(bf16[2,128,256]{2,1,0:T(8,128)(2,1)S(1)} %copy-done.7), channel_id=1, source_target_pairs={{0,16},{16,32},{32,48},{48,0},{1,17},{17,33},{33,49},{49,1},{2,18}... | collective-permute-start | bytes 393224 | tf_op jit(solution)/shard_map/ppermute | solution.py:292
  77.7 11.6 %collective-permute-start.11 = (bf16[2,128,256]{2,1,0:T(8,128)(2,1)S(1)}, bf16[2,128,256]{2,1,0:T(8,128)(2,1)S(1)}, u32[]{:S(2)}, u32[]{:S(2)}) collective-permute-start(bf16[2,128,256]{2,1,0:T(8,128)(2,1)S(1)} %copy-done.7), channel_id=1, source_target_pairs={{0,48},{16,0},{32,16},{48,32},{1,49},{17,1},{33,17},{49,33},{2,50}... | collective-permute-start | bytes 393224 | tf_op jit(solution)/shard_map/ppermute | solution.py:292
  83.7 6.6 %collective-permute-start.8 = (bf16[4,8,16,128]{3,2,1,0:T(8,128)(2,1)S(1)}, bf16[4,8,16,128]{3,2,1,0:T(8,128)(2,1)S(1)}, u32[]{:S(2)}, u32[]{:S(2)}) collective-permute-start(bf16[4,8,16,128]{3,2,1,0:T(8,128)(2,1)S(1)} %bitcast.8), channel_id=1, source_target_pairs={{0,1},{1,0},{2,3},{3,2},{4,5},{5,4},{6,7},{7,6},{8,9},{9,8},{10,11... | collective-permute-start | bytes 393224 | tf_op jit(solution)/shard_map/ppermute | solution.py:278
  90.6 7.7 %collective-permute-start.14 = (bf16[8,2,16,256]{3,2,1,0:T(8,128)(2,1)S(1)}, bf16[8,2,16,256]{3,2,1,0:T(8,128)(2,1)S(1)}, u32[]{:S(2)}, u32[]{:S(2)}) collective-permute-start(bf16[8,2,16,256]{3,2,1,0:T(8,128)(2,1)S(1)} %shard_map.118.p0), channel_id=1, source_target_pairs={{0,192},{64,128},{128,64},{192,0},{1,193},{65,129},{129,65},{193,1... | collective-permute-start | bytes 393224 | tf_op jit(solution)/shard_map/ppermute | solution.py:323
  92.5 6.0 %collective-permute-start.13 = (bf16[8,2,16,256]{3,2,1,0:T(8,128)(2,1)S(1)}, bf16[8,2,16,256]{3,2,1,0:T(8,128)(2,1)S(1)}, u32[]{:S(2)}, u32[]{:S(2)}) collective-permute-start(bf16[8,2,16,256]{3,2,1,0:T(8,128)(2,1)S(1)} %shard_map.118.p0), channel_id=1, source_target_pairs={{0,128},{64,192},{128,0},{192,64},{1,129},{65,193},{129,1},{193,65... | collective-permute-start | bytes 393224 | tf_op jit(solution)/shard_map/ppermute | solution.py:323
  92.8 7.0 %collective-permute-start.12 = (bf16[8,2,16,256]{3,2,1,0:T(8,128)(2,1)S(1)}, bf16[8,2,16,256]{3,2,1,0:T(8,128)(2,1)S(1)}, u32[]{:S(2)}, u32[]{:S(2)}) collective-permute-start(bf16[8,2,16,256]{3,2,1,0:T(8,128)(2,1)S(1)} %shard_map.118.p0), channel_id=1, source_target_pairs={{0,64},{64,0},{128,192},{192,128},{1,65},{65,1},{129,193},{193,129... | collective-permute-start | bytes 393224 | tf_op jit(solution)/shard_map/ppermute | solution.py:323
  93.9 4.4 %collective-permute-start.15 = (bf16[128,256]{1,0:T(8,128)(2,1)S(1)}, bf16[128,256]{1,0:T(8,128)(2,1)S(1)}, u32[]{:S(2)}, u32[]{:S(2)}) collective-permute-start(bf16[128,256]{1,0:T(8,128)(2,1)S(1)} %get-tuple-element.19), channel_id=1, source_target_pairs={{0,1},{1,0},{2,3},{3,2},{4,5},{5,4},{6,7},{7,6},{8,9},{9,8},{10,11... | collective-permute-start | bytes 196616 | tf_op jit(solution)/shard_map/ppermute | solution.py:278

commit v3 on v0

--- a/solution.py
+++ b/solution.py
@@ -145,21 +145,19 @@
     ]
 
 
-def middle_kernel(p0, p1, p2, p3, tok, bundle_a, bundle_b, payload_ref, x_ref):
+def middle_kernel(p0, p1, p2, p3, tok, gain, *refs):
+    w, (bundle, payload_ref, x_ref) = refs[0:4], refs[4:]
     core = lax.axis_index("c")
     n_z, _, own_rows, feats = tok.shape
     rows = n_z * own_rows
     mine = tok[:, core].reshape(rows, feats)
-    halves = add_up((p0, p1, p2, p3), [mine, bundle_b[0:rows, 4 * LANES :]])
-    results = []
-    for half, bundle in zip(halves, (bundle_a, bundle_b)):
-        gain = sum(
-            bundle[rows + 16 * n : rows + 16 * n + 16, 4 * LANES :][0:1].astype(F32)
-            for n in range(3)
-        )
-        weights = [bundle[:, p * LANES : (p + 1) * LANES] for p in range(4)]
-        results.append(project(half, gain, weights))
-    (totals, squares), (others, other_squares) = results
+    halves = add_up((p0, p1, p2, p3), [mine, bundle[0:rows, 4 * LANES :]])
+    other_gain = sum(
+        bundle[rows + 16 * n : rows + 16 * n + 16, 4 * LANES :][0:1].astype(F32) for n in range(3)
+    )
+    totals, squares = project(halves[0], gain[1:2, :], [v[1] for v in w])
+    other_w = [bundle[:, p * LANES : (p + 1) * LANES] for p in range(4)]
+    others, other_squares = project(halves[1], other_gain, other_w)
     store([t + o for t, o in zip(totals, others)], squares + other_squares, payload_ref)
     x_ref[0] = halves[0]
     x_ref[1] = halves[1]
@@ -324,7 +322,7 @@
         if layer == 0:
             payload, x = call(
                 middle_kernel, [payload_shape, x_shape],
-                *parts, tok, bundle, bundle_b, flops=10**8,
+                *parts, tok, norm_gain, *weights, bundle_b, flops=10**8,
             )
     half = jax.ShapeDtypeStruct((rows, feats), BF16)
     keep, send = call(last_kernel, [half, half], *parts, x, flops=10**6)

time: 96.8 us -> 99.5 us (1.028)
  local copies, waits for them, and re-layouts: 2.63 us -> 5.26 us
    unnamed x10 -> x18, local copies, waits for them, and re-layouts: 2.63 us -> 5.26 us
where the time goes in v3:
time: 99.5 us; the launch traced here: 99 us
  starting transfers between devices  37.7 us (38%)
  blocking collectives  22.8 us (23%)
  waiting for transfers between devices  20.7 us (21%)
  Pallas kernels  10.7 us (11%)
  local copies, waits for them, and re-layouts  5.26 us (5%)
    all_to_all x2, blocking collectives, spread(): return lax.all_to_all(copies, axes, split_axis=0, concat_axis=0, tiled=True)  22.8 us
    ppermute x4, starting transfers between devices, swap(): return lax.ppermute(v, 'c', [(0, 1), (1, 0)])  16.3 us
    all_to_all x2, waiting for transfers between devices, spread(): return lax.all_to_all(copies, axes, split_axis=0, concat_axis=0, tiled=True)  12.2 us
    all_to_all x2, starting transfers between devices, spread(): return lax.all_to_all(copies, axes, split_axis=0, concat_axis=0, tiled=True)  11.9 us
    ppermute x6, waiting for transfers between devices, per_device(): parts.append(lax.ppermute(own, 'y', [(i, i ^ k) for i in range(n_y)]))  8.46 us
    ppermute x6, starting transfers between devices, per_device(): parts.append(lax.ppermute(own, 'y', [(i, i ^ k) for i in range(n_y)]))  6.86 us
    unnamed x18, local copies, waits for them, and re-layouts  5.26 us
    pallas_call x8, Pallas kernels, call(): pl.pallas_call(kernel, out_shape=outs, in_specs=[vmem] * len(args), out_s...  4.98 us
  transfers between devices with their start and end apart: 15, of which 7 were waited for; matrix products, arithmetic and copies ran while one was open for 1% of the time, Pallas kernels for 5%

profile of v3, /device:TPU:1, one launch (start us, length us, event | category | flops | bytes accessed | tf_op | source)
XLA Modules:
  0.0 99.0 jit_solution(1146013282229612376)
XLA Ops:
  0.6 0.0 copy-start
  0.6 2.6 %start.1 = (f32[136,640]{1,0:T(8,128)}, bf16[8,16,640]{2,1,0:T(8,128)(2,1)}, bf16[256,768]{1,0:T(8,128)(2,1)}) custom-call(bf16[8,2,16,256]{3,2,1,0:T(8,128)(2,1)} %bitcast.8, f32[2,256]{1,0:T(2,128)} %gain.3, f32[2,128]{1,0:T(2,128)} %floor_rate.1, f32[2,128]{1,0:T(2,128)} %head_gain.1, bf16[2,256,128]{2,1,0:T(8,128)(2,1)} %refs_0_.3, ...), custom_call_target="tpu_custom_call" | custom-call | flops 100000000 | bytes 1000000 | tf_op jit(solution)/shard_map/start/pallas_call | solution.py:107
  3.2 3.3 %collective-permute-start = (bf16[8,16,640]{2,1,0:T(8,128)(2,1)}, bf16[8,16,640]{2,1,0:T(8,128)(2,1)S(1)}, u32[]{:S(2)}, u32[]{:S(2)}) collective-permute-start(bf16[8,16,640]{2,1,0:T(8,128)(2,1)} %get-tuple-element.16), channel_id=1, source_target_pairs={{0,1},{1,0},{2,3},{3,2},{4,5},{5,4},{6,7},{7,6},{8,9},{9,8},{10,11... | collective-permute-start | bytes 491528 | tf_op jit(solution)/shard_map/ppermute | solution.py:280
  6.5 0.0 collective-permute-start.1
  6.5 2.7 %collective-permute-start.3 = (bf16[2,128,256]{2,1,0:T(8,128)(2,1)}, bf16[2,128,256]{2,1,0:T(8,128)(2,1)S(1)}, u32[]{:S(2)}, u32[]{:S(2)}) collective-permute-start(bf16[2,128,256]{2,1,0:T(8,128)(2,1)} %param.18), channel_id=1, source_target_pairs={{0,48},{16,0},{32,16},{48,32},{1,49},{17,1},{33,17},{49,33},{2,50}... | collective-permute-start | bytes 393224 | tf_op jit(solution)/shard_map/ppermute | solution.py:297
  9.2 0.0 collective-permute-start.2
  9.2 0.0 collective-permute-done.received
  9.2 0.0 copy-start.6
  9.2 1.0 copy-done.6
  10.2 0.9 shard_map.113
  11.0 8.0 %all-to-all-start = ((bf16[8,16,640]{2,1,0:T(8,128)(2,1)}), bf16[8,16,640]{2,1,0:T(8,128)(2,1)S(1)}, u32[]{:S(2)}, u32[]{:S(2)}) async-start(bf16[8,16,640]{2,1,0:T(8,128)(2,1)} %get-tuple-element.17), calls=%async_computation | async-start | bytes 327680 | tf_op jit(solution)/shard_map/all_to_all | solution.py:268
  19.0 0.0 collective-permute-done.1
  19.0 0.0 collective-permute-done.3
  19.1 0.0 collective-permute-done.2
  19.1 1.0 pad_maximum_fusion.w_a
  20.0 0.0 copy-start.1
  20.1 0.0 copy-start.8
  20.1 1.3 %collective-permute-start.4 = (bf16[4,2,128,256]{3,2,1,0:T(8,128)(2,1)S(1)}, bf16[4,2,128,256]{3,2,1,0:T(8,128)(2,1)S(1)}, u32[]{:S(2)}, u32[]{:S(2)}) collective-permute-start(bf16[4,2,128,256]{3,2,1,0:T(8,128)(2,1)S(1)} %pad_maximum_fusion.w_a), channel_id=1, source_target_pairs={{0,1},{1,0},{2,3},{3,2},{4,5},{5,4},{6,7},{7,6},{8,9},{9,8},{10,11... | collective-permute-start | bytes 1572872 | tf_op jit(solution)/shard_map/ppermute | solution.py:280
  21.4 5.7 %all-to-all-done.arrived = bf16[8,16,640]{2,1,0:T(8,128)(2,1)S(1)} async-done(((bf16[8,16,640]{2,1,0:T(8,128)(2,1)}), bf16[8,16,640]{2,1,0:T(8,128)(2,1)S(1)}, u32[]{:S(2)}, u32[]{:S(2)}) %all-to-all-start) | async-done | bytes 163872 | tf_op jit(solution)/shard_map/all_to_all | solution.py:268
  27.1 0.0 copy-done
  27.1 0.7 shard_map.114
  27.9 0.0 copy-start.7
  27.9 0.6 copy-done.7
  28.5 3.9 %all-to-all-start.1 = ((bf16[32,16,128]{2,1,0:T(8,128)(2,1)}), bf16[32,16,128]{2,1,0:T(8,128)(2,1)S(1)}, u32[]{:S(2)}, u32[]{:S(2)}) async-start(bf16[32,16,128]{2,1,0:T(8,128)(2,1)} %copy-done.7), calls=%async_computation.1 | async-start | bytes 262144 | tf_op jit(solution)/shard_map/all_to_all | solution.py:268
  32.4 2.7 %collective-permute-start.8 = (bf16[256,768]{1,0:T(8,128)(2,1)}, bf16[256,768]{1,0:T(8,128)(2,1)}, u32[]{:S(2)}, u32[]{:S(2)}) collective-permute-start(bf16[256,768]{1,0:T(8,128)(2,1)} %get-tuple-element.20), channel_id=1, source_target_pairs={{0,1},{1,0},{2,3},{3,2},{4,5},{5,4},{6,7},{7,6},{8,9},{9,8},{10,11... | collective-permute-start | bytes 1179656 | tf_op jit(solution)/shard_map/ppermute | solution.py:280
  35.1 0.0 collective-permute-done.4.w_b
  35.1 6.5 %all-to-all-done.1 = bf16[32,16,128]{2,1,0:T(8,128)(2,1)S(1)} async-done(((bf16[32,16,128]{2,1,0:T(8,128)(2,1)}), bf16[32,16,128]{2,1,0:T(8,128)(2,1)S(1)}, u32[]{:S(2)}, u32[]{:S(2)}) %all-to-all-start.1) | async-done | bytes 131104 | tf_op jit(solution)/shard_map/all_to_all | solution.py:268
  41.6 0.3 shard_map.115.p0
  41.9 2.8 %collective-permute-start.7 = (bf16[128,512]{1,0:T(8,128)(2,1)S(1)}, bf16[128,512]{1,0:T(8,128)(2,1)S(1)}, u32[]{:S(2)}, u32[]{:S(2)}) collective-permute-start(bf16[128,512]{1,0:T(8,128)(2,1)S(1)} %shard_map.115.p0), channel_id=1, source_target_pairs={{0,192},{64,128},{128,64},{192,0},{1,193},{65,129},{129,65},{193,1... | collective-permute-start | bytes 393224 | tf_op jit(solution)/shard_map/ppermute | solution.py:321
  44.8 0.3 collective-permute-start.6
  45.1 0.3 collective-permute-start.5
  45.4 0.0 collective-permute-done.8.refs_4_
  45.4 2.6 %collective-permute-done.7.p3 = bf16[128,512]{1,0:T(8,128)(2,1)S(1)} collective-permute-done((bf16[128,512]{1,0:T(8,128)(2,1)S(1)}, bf16[128,512]{1,0:T(8,128)(2,1)S(1)}, u32[]{:S(2)}, u32[]{:S(2)}) %collective-permute-start.7) | collective-permute-done | bytes 131104 | tf_op jit(solution)/shard_map/ppermute | solution.py:321
  48.1 2.0 %collective-permute-done.6.p2 = bf16[128,512]{1,0:T(8,128)(2,1)S(1)} collective-permute-done((bf16[128,512]{1,0:T(8,128)(2,1)S(1)}, bf16[128,512]{1,0:T(8,128)(2,1)S(1)}, u32[]{:S(2)}, u32[]{:S(2)}) %collective-permute-start.6) | collective-permute-done | bytes 131104 | tf_op jit(solution)/shard_map/ppermute | solution.py:321
  50.1 0.0 collective-permute-done.5.p1
  50.1 0.0 copy-done.1
  50.1 0.0 copy-done.8
  50.1 0.0 copy-start.2
  50.1 0.9 copy-done.2
  51.0 0.0 copy-start.3
  51.0 0.9 copy-done.3
  51.9 0.0 copy-start.4
  51.9 0.9 copy-done.4
  52.8 0.0 copy-start.5
  52.8 0.9 copy-done.5
  53.7 1.3 %shard_map.116 = (bf16[8,16,640]{2,1,0:T(8,128)(2,1)S(1)}, bf16[2,128,256]{2,1,0:T(8,128)(2,1)S(1)}) custom-call(bf16[128,512]{1,0:T(8,128)(2,1)S(1)} %shard_map.115.p0, bf16[128,512]{1,0:T(8,128)(2,1)S(1)} %collective-permute-done.5.p1, bf16[128,512]{1,0:T(8,128)(2,1)S(1)} %collective-permute-done.6.p2, bf16[128,512]{1,0:T(8,128)(2,1)S(1)} %collective-permute-done.7.p3, ...), custom_call_target="tpu_custom_call" | custom-call | flops 100000000 | bytes 1574912 | tf_op jit(solution)/shard_map/pallas_call | solution.py:25
  55.0 10.7 %all_to_all.20.arrived = bf16[8,16,640]{2,1,0:T(8,128)(2,1)S(1)} all-to-all(bf16[8,16,640]{2,1,0:T(8,128)(2,1)S(1)} %get-tuple-element.21), channel_id=1, replica_groups=mesh['y'=4,'x'=4,'z'=8,'c'=2] {'z'}, dimensions={0} | all-to-all | bytes 327680 | tf_op jit(solution)/shard_map/all_to_all | solution.py:268
  65.7 0.7 shard_map.117
  66.5 12.1 %all_to_all.21 = bf16[32,16,128]{2,1,0:T(8,128)(2,1)S(1)} all-to-all(bf16[32,16,128]{2,1,0:T(8,128)(2,1)S(1)} %get-tuple-element.22), channel_id=1, replica_groups=mesh['y'=4,'x'=4,'z'=8,'c'=2] {'x','z'}, dimensions={0} | all-to-all | bytes 262144 | tf_op jit(solution)/shard_map/all_to_all | solution.py:268
  78.6 0.3 shard_map.118.refs_0_
  78.9 1.8 %collective-permute-start.11 = (bf16[128,512]{1,0:T(8,128)(2,1)S(1)}, bf16[128,512]{1,0:T(8,128)(2,1)S(1)}, u32[]{:S(2)}, u32[]{:S(2)}) collective-permute-start(bf16[128,512]{1,0:T(8,128)(2,1)S(1)} %shard_map.118.refs_0_), channel_id=1, source_target_pairs={{0,192},{64,128},{128,64},{192,0},{1,193},{65,129},{129,65},{193,1... | collective-permute-start | bytes 393224 | tf_op jit(solution)/shard_map/ppermute | solution.py:321
  80.6 0.6 collective-permute-start.10
  81.2 1.0 collective-permute-start.9
  82.2 2.1 %collective-permute-done.11.refs_3_ = bf16[128,512]{1,0:T(8,128)(2,1)S(1)} collective-permute-done((bf16[128,512]{1,0:T(8,128)(2,1)S(1)}, bf16[128,512]{1,0:T(8,128)(2,1)S(1)}, u32[]{:S(2)}, u32[]{:S(2)}) %collective-permute-start.11) | collective-permute-done | bytes 131104 | tf_op jit(solution)/shard_map/ppermute | solution.py:321
  84.3 1.7 %collective-permute-done.10.refs_2_ = bf16[128,512]{1,0:T(8,128)(2,1)S(1)} collective-permute-done((bf16[128,512]{1,0:T(8,128)(2,1)S(1)}, bf16[128,512]{1,0:T(8,128)(2,1)S(1)}, u32[]{:S(2)}, u32[]{:S(2)}) %collective-permute-start.10) | collective-permute-done | bytes 131104 | tf_op jit(solution)/shard_map/ppermute | solution.py:321
  86.0 0.1 collective-permute-done.9.refs_1_
  86.0 0.1 shard_map.119
  86.1 9.0 %collective-permute-start.12 = (bf16[128,256]{1,0:T(8,128)(2,1)S(1)}, bf16[128,256]{1,0:T(8,128)(2,1)S(1)}, u32[]{:S(2)}, u32[]{:S(2)}) collective-permute-start(bf16[128,256]{1,0:T(8,128)(2,1)S(1)} %get-tuple-element.25), channel_id=1, source_target_pairs={{0,1},{1,0},{2,3},{3,2},{4,5},{5,4},{6,7},{7,6},{8,9},{9,8},{10,11... | collective-permute-start | bytes 196616 | tf_op jit(solution)/shard_map/ppermute | solution.py:280
  95.1 3.2 %new_states.1 = f32[2,16,1,128,128]{4,3,2,1,0:T(8,128)} custom-call(f32[3,16,128]{2,1,0:T(8,128)S(1)} %get-tuple-element.26.terms_a, f32[3,16,128]{2,1,0:T(8,128)S(1)} %get-tuple-element.27.terms_b, f32[2,16,1,128,128]{4,3,2,1,0:T(8,128)S(1)} %copy-done), custom_call_target="tpu_custom_call" | custom-call | flops 10000000 | bytes 4194304 | tf_op jit(solution)/shard_map/new_states/pallas_call | solution.py:238
  98.3 0.0 collective-permute-done.12.received
  98.3 0.7 shard_map.120
Async XLA Ops:
  0.6 26.5 %copy-start = (f32[2,16,1,128,128]{4,3,2,1,0:T(8,128)S(1)}, f32[2,16,1,128,128]{4,3,2,1,0:T(8,128)}, u32[]{:S(2)}) copy-start(f32[2,16,1,128,128]{4,3,2,1,0:T(8,128)} %state.5) | copy-start | bytes 6291460
  3.2 6.0 %collective-permute-start = (bf16[8,16,640]{2,1,0:T(8,128)(2,1)}, bf16[8,16,640]{2,1,0:T(8,128)(2,1)S(1)}, u32[]{:S(2)}, u32[]{:S(2)}) collective-permute-start(bf16[8,16,640]{2,1,0:T(8,128)(2,1)} %get-tuple-element.16), channel_id=1, source_target_pairs={{0,1},{1,0},{2,3},{3,2},{4,5},{5,4},{6,7},{7,6},{8,9},{9,8},{10,11... | collective-permute-start | bytes 491528 | tf_op jit(solution)/shard_map/ppermute | solution.py:280
  6.5 12.5 %collective-permute-start.1 = (bf16[2,128,256]{2,1,0:T(8,128)(2,1)}, bf16[2,128,256]{2,1,0:T(8,128)(2,1)S(1)}, u32[]{:S(2)}, u32[]{:S(2)}) collective-permute-start(bf16[2,128,256]{2,1,0:T(8,128)(2,1)} %param.18), channel_id=1, source_target_pairs={{0,16},{16,32},{32,48},{48,0},{1,17},{17,33},{33,49},{49,1},{2,18}... | collective-permute-start | bytes 393224 | tf_op jit(solution)/shard_map/ppermute | solution.py:297
  6.5 12.5 %collective-permute-start.3 = (bf16[2,128,256]{2,1,0:T(8,128)(2,1)}, bf16[2,128,256]{2,1,0:T(8,128)(2,1)S(1)}, u32[]{:S(2)}, u32[]{:S(2)}) collective-permute-start(bf16[2,128,256]{2,1,0:T(8,128)(2,1)} %param.18), channel_id=1, source_target_pairs={{0,48},{16,0},{32,16},{48,32},{1,49},{17,1},{33,17},{49,33},{2,50}... | collective-permute-start | bytes 393224 | tf_op jit(solution)/shard_map/ppermute | solution.py:297
  9.2 9.9 %collective-permute-start.2 = (bf16[2,128,256]{2,1,0:T(8,128)(2,1)}, bf16[2,128,256]{2,1,0:T(8,128)(2,1)S(1)}, u32[]{:S(2)}, u32[]{:S(2)}) collective-permute-start(bf16[2,128,256]{2,1,0:T(8,128)(2,1)} %param.18), channel_id=1, source_target_pairs={{0,32},{16,48},{32,0},{48,16},{1,33},{17,49},{33,1},{49,17},{2,34}... | collective-permute-start | bytes 393224 | tf_op jit(solution)/shard_map/ppermute | solution.py:297
  9.2 1.0 copy-start.6
  11.0 16.1 %all-to-all-start = ((bf16[8,16,640]{2,1,0:T(8,128)(2,1)}), bf16[8,16,640]{2,1,0:T(8,128)(2,1)S(1)}, u32[]{:S(2)}, u32[]{:S(2)}) async-start(bf16[8,16,640]{2,1,0:T(8,128)(2,1)} %get-tuple-element.17), calls=%async_computation | async-start | bytes 327680 | tf_op jit(solution)/shard_map/all_to_all | solution.py:268
  20.0 30.1 %copy-start.1 = (bf16[256,256]{1,0:T(8,128)(2,1)S(1)}, bf16[256,256]{1,0:T(8,128)(2,1)}, u32[]{:S(2)}) copy-start(bf16[256,256]{1,0:T(8,128)(2,1)} %param.10) | copy-start | bytes 393220
  20.1 30.0 %copy-start.8 = (f32[2,256]{1,0:T(2,128)S(1)}, f32[2,256]{1,0:T(2,128)}, u32[]{:S(2)}) copy-start(f32[2,256]{1,0:T(2,128)} %gain.3) | copy-start | bytes 6148
  20.1 15.1 %collective-permute-start.4 = (bf16[4,2,128,256]{3,2,1,0:T(8,128)(2,1)S(1)}, bf16[4,2,128,256]{3,2,1,0:T(8,128)(2,1)S(1)}, u32[]{:S(2)}, u32[]{:S(2)}) collective-permute-start(bf16[4,2,128,256]{3,2,1,0:T(8,128)(2,1)S(1)} %pad_maximum_fusion.w_a), channel_id=1, source_target_pairs={{0,1},{1,0},{2,3},{3,2},{4,5},{5,4},{6,7},{7,6},{8,9},{9,8},{10,11... | collective-permute-start | bytes 1572872 | tf_op jit(solution)/shard_map/ppermute | solution.py:280
  27.9 0.7 copy-start.7
  28.5 13.1 %all-to-all-start.1 = ((bf16[32,16,128]{2,1,0:T(8,128)(2,1)}), bf16[32,16,128]{2,1,0:T(8,128)(2,1)S(1)}, u32[]{:S(2)}, u32[]{:S(2)}) async-start(bf16[32,16,128]{2,1,0:T(8,128)(2,1)} %copy-done.7), calls=%async_computation.1 | async-start | bytes 262144 | tf_op jit(solution)/shard_map/all_to_all | solution.py:268
  32.4 13.1 %collective-permute-start.8 = (bf16[256,768]{1,0:T(8,128)(2,1)}, bf16[256,768]{1,0:T(8,128)(2,1)}, u32[]{:S(2)}, u32[]{:S(2)}) collective-permute-start(bf16[256,768]{1,0:T(8,128)(2,1)} %get-tuple-element.20), channel_id=1, source_target_pairs={{0,1},{1,0},{2,3},{3,2},{4,5},{5,4},{6,7},{7,6},{8,9},{9,8},{10,11... | collective-permute-start | bytes 1179656 | tf_op jit(solution)/shard_map/ppermute | solution.py:280
  41.9 6.2 %collective-permute-start.7 = (bf16[128,512]{1,0:T(8,128)(2,1)S(1)}, bf16[128,512]{1,0:T(8,128)(2,1)S(1)}, u32[]{:S(2)}, u32[]{:S(2)}) collective-permute-start(bf16[128,512]{1,0:T(8,128)(2,1)S(1)} %shard_map.115.p0), channel_id=1, source_target_pairs={{0,192},{64,128},{128,64},{192,0},{1,193},{65,129},{129,65},{193,1... | collective-permute-start | bytes 393224 | tf_op jit(solution)/shard_map/ppermute | solution.py:321
  44.8 5.3 %collective-permute-start.6 = (bf16[128,512]{1,0:T(8,128)(2,1)S(1)}, bf16[128,512]{1,0:T(8,128)(2,1)S(1)}, u32[]{:S(2)}, u32[]{:S(2)}) collective-permute-start(bf16[128,512]{1,0:T(8,128)(2,1)S(1)} %shard_map.115.p0), channel_id=1, source_target_pairs={{0,128},{64,192},{128,0},{192,64},{1,129},{65,193},{129,1},{193,65... | collective-permute-start | bytes 393224 | tf_op jit(solution)/shard_map/ppermute | solution.py:321
  45.1 5.0 %collective-permute-start.5 = (bf16[128,512]{1,0:T(8,128)(2,1)S(1)}, bf16[128,512]{1,0:T(8,128)(2,1)S(1)}, u32[]{:S(2)}, u32[]{:S(2)}) collective-permute-start(bf16[128,512]{1,0:T(8,128)(2,1)S(1)} %shard_map.115.p0), channel_id=1, source_target_pairs={{0,64},{64,0},{128,192},{192,128},{1,65},{65,1},{129,193},{193,129... | collective-permute-start | bytes 393224 | tf_op jit(solution)/shard_map/ppermute | solution.py:321
  50.1 0.9 copy-start.2
  51.0 0.9 copy-start.3
  51.9 0.9 copy-start.4
  52.8 0.9 copy-start.5
  78.9 5.4 %collective-permute-start.11 = (bf16[128,512]{1,0:T(8,128)(2,1)S(1)}, bf16[128,512]{1,0:T(8,128)(2,1)S(1)}, u32[]{:S(2)}, u32[]{:S(2)}) collective-permute-start(bf16[128,512]{1,0:T(8,128)(2,1)S(1)} %shard_map.118.refs_0_), channel_id=1, source_target_pairs={{0,192},{64,128},{128,64},{192,0},{1,193},{65,129},{129,65},{193,1... | collective-permute-start | bytes 393224 | tf_op jit(solution)/shard_map/ppermute | solution.py:321
  80.6 5.3 %collective-permute-start.10 = (bf16[128,512]{1,0:T(8,128)(2,1)S(1)}, bf16[128,512]{1,0:T(8,128)(2,1)S(1)}, u32[]{:S(2)}, u32[]{:S(2)}) collective-permute-start(bf16[128,512]{1,0:T(8,128)(2,1)S(1)} %shard_map.118.refs_0_), channel_id=1, source_target_pairs={{0,128},{64,192},{128,0},{192,64},{1,129},{65,193},{129,1},{193,65... | collective-permute-start | bytes 393224 | tf_op jit(solution)/shard_map/ppermute | solution.py:321
  81.2 4.8 %collective-permute-start.9 = (bf16[128,512]{1,0:T(8,128)(2,1)S(1)}, bf16[128,512]{1,0:T(8,128)(2,1)S(1)}, u32[]{:S(2)}, u32[]{:S(2)}) collective-permute-start(bf16[128,512]{1,0:T(8,128)(2,1)S(1)} %shard_map.118.refs_0_), channel_id=1, source_target_pairs={{0,64},{64,0},{128,192},{192,128},{1,65},{65,1},{129,193},{193,129... | collective-permute-start | bytes 393224 | tf_op jit(solution)/shard_map/ppermute | solution.py:321
  86.1 12.2 %collective-permute-start.12 = (bf16[128,256]{1,0:T(8,128)(2,1)S(1)}, bf16[128,256]{1,0:T(8,128)(2,1)S(1)}, u32[]{:S(2)}, u32[]{:S(2)}) collective-permute-start(bf16[128,256]{1,0:T(8,128)(2,1)S(1)} %get-tuple-element.25), channel_id=1, source_target_pairs={{0,1},{1,0},{2,3},{3,2},{4,5},{5,4},{6,7},{7,6},{8,9},{9,8},{10,11... | collective-permute-start | bytes 196616 | tf_op jit(solution)/shard_map/ppermute | solution.py:280

commit v4 on v3

--- a/solution.py
+++ b/solution.py
@@ -120,19 +120,32 @@
             pltpu.VMEM((4, *own[4].shape), BF16),
             pltpu.SemaphoreType.DMA((8,)),
         ],
-        cost_estimate=pl.CostEstimate(flops=10**8, bytes_accessed=10**6, transcendentals=0),
+        cost_estimate=pl.CostEstimate(flops=10**9, bytes_accessed=10**6, transcendentals=0),
         compiler_params=pltpu.CompilerParams(vmem_limit_bytes=START_LIMIT),
         name="start",
     )(*own)
 
 
-def pair_kernel(keep, received, payload_ref, rates_ref):
+def lanes_kernel(out_ref):
+    row = lax.broadcasted_iota(jnp.int32, out_ref.shape, 0)
+    lane = lax.broadcasted_iota(jnp.int32, out_ref.shape, 1)
+    out_ref[...] = jnp.where(row == lane, 1.0, 0.0)
+
+
+def pair_kernel(keep, received, lanes, payload_ref, rates_ref):
     n_z, own_rows, width = received.shape
     rates_ref[...] = keep[n_z * own_rows :, 0:LANES]
     total = keep[0 : n_z * own_rows, :] + received[...].reshape(n_z * own_rows, width).astype(F32)
     extra = total[:, 4 * LANES :]
     squares = extra[:, 0:1] + extra[:, 1:2] + extra[:, 2:3]
-    store([total[:, p * LANES : (p + 1) * LANES] for p in range(4)], squares, payload_ref)
+    for p in range(4):
+        payload_ref[:, :, p * LANES : (p + 1) * LANES] = (
+            total[:, p * LANES : (p + 1) * LANES].astype(BF16).reshape(n_z, own_rows, LANES)
+        )
+    high = rounded(squares)
+    middle = rounded(squares - high)
+    terms = high * lanes[0:1] + middle * lanes[1:2] + (squares - high - middle) * lanes[2:3]
+    payload_ref[:, :, 4 * LANES :] = terms.astype(BF16).reshape(n_z, own_rows, LANES)
 
 
 def add_up(parts, halves):
@@ -287,9 +300,10 @@
         payload_shape, rows, tok, norm_gain, floor_rate, head_gain, *weights
     )
     received = swap(send)
+    (lanes,) = call(lanes_kernel, [jax.ShapeDtypeStruct((8, LANES), F32)], flops=10**9)
     payload, rates = call(
         pair_kernel, [payload_shape, jax.ShapeDtypeStruct((8, LANES), F32)],
-        keep, received, flops=10**6,
+        keep, received, lanes, flops=10**6,
     )
     bundle_b = swap(bundle)
     pieces = [w_output]

time: 99.5 us -> 98.4 us (0.989)
    unnamed x18 -> x20, local copies, waits for them, and re-layouts: 5.26 us -> 4.29 us
    pallas_call x8 -> x9, Pallas kernels: 4.98 us -> 4.99 us  [call(): pl.pallas_call(kernel, out_shape=outs, in_specs=[vmem] * len(args), out_s...]
  transfers between devices with their start and end apart: 15 -> 15, of which waited for: 7 -> 7; matrix products, arithmetic and copies ran while one was open for 1% -> 0% of each run, Pallas kernels for 5% -> 5%
where the time goes in v4:
time: 98.4 us; the launch traced here: 97.9 us
  starting transfers between devices  37.8 us (38%)
  blocking collectives  22.8 us (23%)
  waiting for transfers between devices  21.6 us (22%)
  Pallas kernels  10.6 us (11%)
  local copies, waits for them, and re-layouts  4.29 us (4%)
    all_to_all x2, blocking collectives, spread(): return lax.all_to_all(copies, axes, split_axis=0, concat_axis=0, tiled=True)  22.8 us
    ppermute x4, starting transfers between devices, swap(): return lax.ppermute(v, 'c', [(0, 1), (1, 0)])  16.4 us
    all_to_all x2, waiting for transfers between devices, spread(): return lax.all_to_all(copies, axes, split_axis=0, concat_axis=0, tiled=True)  13.1 us
    all_to_all x2, starting transfers between devices, spread(): return lax.all_to_all(copies, axes, split_axis=0, concat_axis=0, tiled=True)  11.9 us
    ppermute x6, waiting for transfers between devices, per_device(): parts.append(lax.ppermute(own, 'y', [(i, i ^ k) for i in range(n_y)]))  8.45 us
    ppermute x6, starting transfers between devices, per_device(): parts.append(lax.ppermute(own, 'y', [(i, i ^ k) for i in range(n_y)]))  6.84 us
    pallas_call x9, Pallas kernels, call(): pl.pallas_call(kernel, out_shape=outs, in_specs=[vmem] * len(args), out_s...  4.99 us
    unnamed x20, local copies, waits for them, and re-layouts  4.29 us
  transfers between devices with their start and end apart: 15, of which 7 were waited for; matrix products, arithmetic and copies ran while one was open for 0% of the time, Pallas kernels for 5%

profile of v4, /device:TPU:1, one launch (start us, length us, event | category | flops | bytes accessed | tf_op | source)
XLA Modules:
  0.0 97.9 jit_solution(18205512796379283658)
XLA Ops:
  0.6 0.0 copy-start.9
  0.6 2.5 %start.1 = (f32[136,640]{1,0:T(8,128)}, bf16[8,16,640]{2,1,0:T(8,128)(2,1)}, bf16[256,768]{1,0:T(8,128)(2,1)}) custom-call(bf16[8,2,16,256]{3,2,1,0:T(8,128)(2,1)} %bitcast.10, f32[2,256]{1,0:T(2,128)} %gain.3, f32[2,128]{1,0:T(2,128)} %floor_rate.1, f32[2,128]{1,0:T(2,128)} %head_gain.1, bf16[2,256,128]{2,1,0:T(8,128)(2,1)} %refs_0_.3, ...), custom_call_target="tpu_custom_call" | custom-call | flops 1000000000 | bytes 1000000 | tf_op jit(solution)/shard_map/start/pallas_call | solution.py:107
  3.1 0.0 copy-start.1
  3.1 0.0 copy-start
  3.1 3.3 %collective-permute-start = (bf16[8,16,640]{2,1,0:T(8,128)(2,1)}, bf16[8,16,640]{2,1,0:T(8,128)(2,1)S(1)}, u32[]{:S(2)}, u32[]{:S(2)}) collective-permute-start(bf16[8,16,640]{2,1,0:T(8,128)(2,1)} %get-tuple-element.16), channel_id=1, source_target_pairs={{0,1},{1,0},{2,3},{3,2},{4,5},{5,4},{6,7},{7,6},{8,9},{9,8},{10,11... | collective-permute-start | bytes 491528 | tf_op jit(solution)/shard_map/ppermute | solution.py:293
  6.4 0.0 copy-done.9
  6.4 0.0 collective-permute-start.1
  6.4 2.7 %collective-permute-start.3 = (bf16[2,128,256]{2,1,0:T(8,128)(2,1)S(1)}, bf16[2,128,256]{2,1,0:T(8,128)(2,1)S(1)}, u32[]{:S(2)}, u32[]{:S(2)}) collective-permute-start(bf16[2,128,256]{2,1,0:T(8,128)(2,1)S(1)} %copy-done.9), channel_id=1, source_target_pairs={{0,48},{16,0},{32,16},{48,32},{1,49},{17,1},{33,17},{49,33},{2,50}... | collective-permute-start | bytes 393224 | tf_op jit(solution)/shard_map/ppermute | solution.py:311
  9.1 0.0 collective-permute-start.2
  9.1 0.0 collective-permute-done.received
  9.1 0.0 copy-done.1
  9.1 0.9 shard_map.114
  10.0 8.0 %all-to-all-start = ((bf16[8,16,640]{2,1,0:T(8,128)(2,1)}), bf16[8,16,640]{2,1,0:T(8,128)(2,1)S(1)}, u32[]{:S(2)}, u32[]{:S(2)}) async-start(bf16[8,16,640]{2,1,0:T(8,128)(2,1)} %get-tuple-element.17), calls=%async_computation | async-start | bytes 327680 | tf_op jit(solution)/shard_map/all_to_all | solution.py:281
  18.0 0.0 collective-permute-done.1
  18.0 0.0 collective-permute-done.3
  18.0 0.0 collective-permute-done.2
  18.0 0.1 pad_maximum_fusion.w_a
  18.1 0.0 copy-start.2
  18.1 0.0 copy-start.8
  18.1 1.3 %collective-permute-start.4 = (bf16[4,2,128,256]{3,2,1,0:T(8,128)(2,1)S(1)}, bf16[4,2,128,256]{3,2,1,0:T(8,128)(2,1)S(1)}, u32[]{:S(2)}, u32[]{:S(2)}) collective-permute-start(bf16[4,2,128,256]{3,2,1,0:T(8,128)(2,1)S(1)} %pad_maximum_fusion.w_a), channel_id=1, source_target_pairs={{0,1},{1,0},{2,3},{3,2},{4,5},{5,4},{6,7},{7,6},{8,9},{9,8},{10,11... | collective-permute-start | bytes 1572872 | tf_op jit(solution)/shard_map/ppermute | solution.py:293
  19.4 6.6 %all-to-all-done.arrived = bf16[8,16,640]{2,1,0:T(8,128)(2,1)S(1)} async-done(((bf16[8,16,640]{2,1,0:T(8,128)(2,1)}), bf16[8,16,640]{2,1,0:T(8,128)(2,1)S(1)}, u32[]{:S(2)}, u32[]{:S(2)}) %all-to-all-start) | async-done | bytes 163872 | tf_op jit(solution)/shard_map/all_to_all | solution.py:281
  26.1 0.0 copy-done
  26.1 0.7 shard_map.115
  26.8 0.0 copy-start.7
  26.8 0.6 copy-done.7
  27.5 3.9 %all-to-all-start.1 = ((bf16[32,16,128]{2,1,0:T(8,128)(2,1)}), bf16[32,16,128]{2,1,0:T(8,128)(2,1)S(1)}, u32[]{:S(2)}, u32[]{:S(2)}) async-start(bf16[32,16,128]{2,1,0:T(8,128)(2,1)} %copy-done.7), calls=%async_computation.1 | async-start | bytes 262144 | tf_op jit(solution)/shard_map/all_to_all | solution.py:281
  31.3 2.7 %collective-permute-start.8 = (bf16[256,768]{1,0:T(8,128)(2,1)}, bf16[256,768]{1,0:T(8,128)(2,1)}, u32[]{:S(2)}, u32[]{:S(2)}) collective-permute-start(bf16[256,768]{1,0:T(8,128)(2,1)} %get-tuple-element.20), channel_id=1, source_target_pairs={{0,1},{1,0},{2,3},{3,2},{4,5},{5,4},{6,7},{7,6},{8,9},{9,8},{10,11... | collective-permute-start | bytes 1179656 | tf_op jit(solution)/shard_map/ppermute | solution.py:293
  34.1 0.0 collective-permute-done.4.w_b
  34.1 6.5 %all-to-all-done.1 = bf16[32,16,128]{2,1,0:T(8,128)(2,1)S(1)} async-done(((bf16[32,16,128]{2,1,0:T(8,128)(2,1)}), bf16[32,16,128]{2,1,0:T(8,128)(2,1)S(1)}, u32[]{:S(2)}, u32[]{:S(2)}) %all-to-all-start.1) | async-done | bytes 131104 | tf_op jit(solution)/shard_map/all_to_all | solution.py:281
  40.6 0.3 shard_map.116.p0
  40.9 2.8 %collective-permute-start.7 = (bf16[128,512]{1,0:T(8,128)(2,1)S(1)}, bf16[128,512]{1,0:T(8,128)(2,1)S(1)}, u32[]{:S(2)}, u32[]{:S(2)}) collective-permute-start(bf16[128,512]{1,0:T(8,128)(2,1)S(1)} %shard_map.116.p0), channel_id=1, source_target_pairs={{0,192},{64,128},{128,64},{192,0},{1,193},{65,129},{129,65},{193,1... | collective-permute-start | bytes 393224 | tf_op jit(solution)/shard_map/ppermute | solution.py:335
  43.7 0.3 collective-permute-start.6
  44.0 0.3 collective-permute-start.5
  44.4 0.0 collective-permute-done.8.refs_4_
  44.4 2.6 %collective-permute-done.7.p3 = bf16[128,512]{1,0:T(8,128)(2,1)S(1)} collective-permute-done((bf16[128,512]{1,0:T(8,128)(2,1)S(1)}, bf16[128,512]{1,0:T(8,128)(2,1)S(1)}, u32[]{:S(2)}, u32[]{:S(2)}) %collective-permute-start.7) | collective-permute-done | bytes 131104 | tf_op jit(solution)/shard_map/ppermute | solution.py:335
  47.0 2.0 %collective-permute-done.6.p2 = bf16[128,512]{1,0:T(8,128)(2,1)S(1)} collective-permute-done((bf16[128,512]{1,0:T(8,128)(2,1)S(1)}, bf16[128,512]{1,0:T(8,128)(2,1)S(1)}, u32[]{:S(2)}, u32[]{:S(2)}) %collective-permute-start.6) | collective-permute-done | bytes 131104 | tf_op jit(solution)/shard_map/ppermute | solution.py:335
  49.0 0.0 collective-permute-done.5.p1
  49.0 0.0 copy-done.2
  49.0 0.0 copy-done.8
  49.0 0.0 copy-start.3
  49.1 0.9 copy-done.3
  49.9 0.0 copy-start.4
  50.0 0.9 copy-done.4
  50.9 0.0 copy-start.5
  50.9 0.9 copy-done.5
  51.8 0.0 copy-start.6
  51.8 0.9 copy-done.6
  52.7 1.3 %shard_map.117 = (bf16[8,16,640]{2,1,0:T(8,128)(2,1)S(1)}, bf16[2,128,256]{2,1,0:T(8,128)(2,1)S(1)}) custom-call(bf16[128,512]{1,0:T(8,128)(2,1)S(1)} %shard_map.116.p0, bf16[128,512]{1,0:T(8,128)(2,1)S(1)} %collective-permute-done.5.p1, bf16[128,512]{1,0:T(8,128)(2,1)S(1)} %collective-permute-done.6.p2, bf16[128,512]{1,0:T(8,128)(2,1)S(1)} %collective-permute-done.7.p3, ...), custom_call_target="tpu_custom_call" | custom-call | flops 100000000 | bytes 1574912 | tf_op jit(solution)/shard_map/pallas_call | solution.py:25
  54.0 10.7 %all_to_all.20.arrived = bf16[8,16,640]{2,1,0:T(8,128)(2,1)S(1)} all-to-all(bf16[8,16,640]{2,1,0:T(8,128)(2,1)S(1)} %get-tuple-element.21), channel_id=1, replica_groups=mesh['y'=4,'x'=4,'z'=8,'c'=2] {'z'}, dimensions={0} | all-to-all | bytes 327680 | tf_op jit(solution)/shard_map/all_to_all | solution.py:281
  64.6 0.7 shard_map.118
  65.4 12.1 %all_to_all.21 = bf16[32,16,128]{2,1,0:T(8,128)(2,1)S(1)} all-to-all(bf16[32,16,128]{2,1,0:T(8,128)(2,1)S(1)} %get-tuple-element.22), channel_id=1, replica_groups=mesh['y'=4,'x'=4,'z'=8,'c'=2] {'x','z'}, dimensions={0} | all-to-all | bytes 262144 | tf_op jit(solution)/shard_map/all_to_all | solution.py:281
  77.5 0.3 shard_map.119.refs_0_
  77.8 1.8 %collective-permute-start.11 = (bf16[128,512]{1,0:T(8,128)(2,1)S(1)}, bf16[128,512]{1,0:T(8,128)(2,1)S(1)}, u32[]{:S(2)}, u32[]{:S(2)}) collective-permute-start(bf16[128,512]{1,0:T(8,128)(2,1)S(1)} %shard_map.119.refs_0_), channel_id=1, source_target_pairs={{0,192},{64,128},{128,64},{192,0},{1,193},{65,129},{129,65},{193,1... | collective-permute-start | bytes 393224 | tf_op jit(solution)/shard_map/ppermute | solution.py:335
  79.6 0.6 collective-permute-start.10
  80.2 0.9 collective-permute-start.9
  81.1 2.1 %collective-permute-done.11.refs_3_ = bf16[128,512]{1,0:T(8,128)(2,1)S(1)} collective-permute-done((bf16[128,512]{1,0:T(8,128)(2,1)S(1)}, bf16[128,512]{1,0:T(8,128)(2,1)S(1)}, u32[]{:S(2)}, u32[]{:S(2)}) %collective-permute-start.11) | collective-permute-done | bytes 131104 | tf_op jit(solution)/shard_map/ppermute | solution.py:335
  83.2 1.7 %collective-permute-done.10.refs_2_ = bf16[128,512]{1,0:T(8,128)(2,1)S(1)} collective-permute-done((bf16[128,512]{1,0:T(8,128)(2,1)S(1)}, bf16[128,512]{1,0:T(8,128)(2,1)S(1)}, u32[]{:S(2)}, u32[]{:S(2)}) %collective-permute-start.10) | collective-permute-done | bytes 131104 | tf_op jit(solution)/shard_map/ppermute | solution.py:335
  84.9 0.1 collective-permute-done.9.refs_1_
  84.9 0.1 shard_map.120
  85.0 9.0 %collective-permute-start.12 = (bf16[128,256]{1,0:T(8,128)(2,1)S(1)}, bf16[128,256]{1,0:T(8,128)(2,1)S(1)}, u32[]{:S(2)}, u32[]{:S(2)}) collective-permute-start(bf16[128,256]{1,0:T(8,128)(2,1)S(1)} %get-tuple-element.25), channel_id=1, source_target_pairs={{0,1},{1,0},{2,3},{3,2},{4,5},{5,4},{6,7},{7,6},{8,9},{9,8},{10,11... | collective-permute-start | bytes 196616 | tf_op jit(solution)/shard_map/ppermute | solution.py:293
  94.1 3.2 %new_states.1 = f32[2,16,1,128,128]{4,3,2,1,0:T(8,128)} custom-call(f32[3,16,128]{2,1,0:T(8,128)S(1)} %get-tuple-element.26.terms_a, f32[3,16,128]{2,1,0:T(8,128)S(1)} %get-tuple-element.27.terms_b, f32[2,16,1,128,128]{4,3,2,1,0:T(8,128)S(1)} %copy-done), custom_call_target="tpu_custom_call" | custom-call | flops 10000000 | bytes 4194304 | tf_op jit(solution)/shard_map/new_states/pallas_call | solution.py:251
  97.2 0.0 collective-permute-done.12.received
  97.2 0.7 shard_map.121
  (1 shorter events, 0.0 us)
Async XLA Ops:
  0.6 5.8 %copy-start.9 = (bf16[2,128,256]{2,1,0:T(8,128)(2,1)S(1)}, bf16[2,128,256]{2,1,0:T(8,128)(2,1)}, u32[]{:S(2)}) copy-start(bf16[2,128,256]{2,1,0:T(8,128)(2,1)} %param.18) | copy-start | bytes 393220
  3.1 6.0 %copy-start.1 = (f32[136,640]{1,0:T(8,128)S(1)}, f32[136,640]{1,0:T(8,128)}, u32[]{:S(2)}) copy-start(f32[136,640]{1,0:T(8,128)} %get-tuple-element.15.keep) | copy-start | bytes 1044484
  3.1 22.9 %copy-start = (f32[2,16,1,128,128]{4,3,2,1,0:T(8,128)S(1)}, f32[2,16,1,128,128]{4,3,2,1,0:T(8,128)}, u32[]{:S(2)}) copy-start(f32[2,16,1,128,128]{4,3,2,1,0:T(8,128)} %state.5) | copy-start | bytes 6291460
  3.1 6.0 %collective-permute-start = (bf16[8,16,640]{2,1,0:T(8,128)(2,1)}, bf16[8,16,640]{2,1,0:T(8,128)(2,1)S(1)}, u32[]{:S(2)}, u32[]{:S(2)}) collective-permute-start(bf16[8,16,640]{2,1,0:T(8,128)(2,1)} %get-tuple-element.16), channel_id=1, source_target_pairs={{0,1},{1,0},{2,3},{3,2},{4,5},{5,4},{6,7},{7,6},{8,9},{9,8},{10,11... | collective-permute-start | bytes 491528 | tf_op jit(solution)/shard_map/ppermute | solution.py:293
  6.4 11.6 %collective-permute-start.1 = (bf16[2,128,256]{2,1,0:T(8,128)(2,1)S(1)}, bf16[2,128,256]{2,1,0:T(8,128)(2,1)S(1)}, u32[]{:S(2)}, u32[]{:S(2)}) collective-permute-start(bf16[2,128,256]{2,1,0:T(8,128)(2,1)S(1)} %copy-done.9), channel_id=1, source_target_pairs={{0,16},{16,32},{32,48},{48,0},{1,17},{17,33},{33,49},{49,1},{2,18}... | collective-permute-start | bytes 393224 | tf_op jit(solution)/shard_map/ppermute | solution.py:311
  6.4 11.6 %collective-permute-start.3 = (bf16[2,128,256]{2,1,0:T(8,128)(2,1)S(1)}, bf16[2,128,256]{2,1,0:T(8,128)(2,1)S(1)}, u32[]{:S(2)}, u32[]{:S(2)}) collective-permute-start(bf16[2,128,256]{2,1,0:T(8,128)(2,1)S(1)} %copy-done.9), channel_id=1, source_target_pairs={{0,48},{16,0},{32,16},{48,32},{1,49},{17,1},{33,17},{49,33},{2,50}... | collective-permute-start | bytes 393224 | tf_op jit(solution)/shard_map/ppermute | solution.py:311
  9.1 8.9 %collective-permute-start.2 = (bf16[2,128,256]{2,1,0:T(8,128)(2,1)S(1)}, bf16[2,128,256]{2,1,0:T(8,128)(2,1)S(1)}, u32[]{:S(2)}, u32[]{:S(2)}) collective-permute-start(bf16[2,128,256]{2,1,0:T(8,128)(2,1)S(1)} %copy-done.9), channel_id=1, source_target_pairs={{0,32},{16,48},{32,0},{48,16},{1,33},{17,49},{33,1},{49,17},{2,34}... | collective-permute-start | bytes 393224 | tf_op jit(solution)/shard_map/ppermute | solution.py:311
  10.0 16.1 %all-to-all-start = ((bf16[8,16,640]{2,1,0:T(8,128)(2,1)}), bf16[8,16,640]{2,1,0:T(8,128)(2,1)S(1)}, u32[]{:S(2)}, u32[]{:S(2)}) async-start(bf16[8,16,640]{2,1,0:T(8,128)(2,1)} %get-tuple-element.17), calls=%async_computation | async-start | bytes 327680 | tf_op jit(solution)/shard_map/all_to_all | solution.py:281
  18.1 30.9 %copy-start.2 = (bf16[256,256]{1,0:T(8,128)(2,1)S(1)}, bf16[256,256]{1,0:T(8,128)(2,1)}, u32[]{:S(2)}) copy-start(bf16[256,256]{1,0:T(8,128)(2,1)} %param.10) | copy-start | bytes 393220
  18.1 30.9 %copy-start.8 = (f32[2,256]{1,0:T(2,128)S(1)}, f32[2,256]{1,0:T(2,128)}, u32[]{:S(2)}) copy-start(f32[2,256]{1,0:T(2,128)} %gain.3) | copy-start | bytes 6148
  18.1 16.0 %collective-permute-start.4 = (bf16[4,2,128,256]{3,2,1,0:T(8,128)(2,1)S(1)}, bf16[4,2,128,256]{3,2,1,0:T(8,128)(2,1)S(1)}, u32[]{:S(2)}, u32[]{:S(2)}) collective-permute-start(bf16[4,2,128,256]{3,2,1,0:T(8,128)(2,1)S(1)} %pad_maximum_fusion.w_a), channel_id=1, source_target_pairs={{0,1},{1,0},{2,3},{3,2},{4,5},{5,4},{6,7},{7,6},{8,9},{9,8},{10,11... | collective-permute-start | bytes 1572872 | tf_op jit(solution)/shard_map/ppermute | solution.py:293
  26.8 0.7 copy-start.7
  27.5 13.1 %all-to-all-start.1 = ((bf16[32,16,128]{2,1,0:T(8,128)(2,1)}), bf16[32,16,128]{2,1,0:T(8,128)(2,1)S(1)}, u32[]{:S(2)}, u32[]{:S(2)}) async-start(bf16[32,16,128]{2,1,0:T(8,128)(2,1)} %copy-done.7), calls=%async_computation.1 | async-start | bytes 262144 | tf_op jit(solution)/shard_map/all_to_all | solution.py:281
  31.3 13.0 %collective-permute-start.8 = (bf16[256,768]{1,0:T(8,128)(2,1)}, bf16[256,768]{1,0:T(8,128)(2,1)}, u32[]{:S(2)}, u32[]{:S(2)}) collective-permute-start(bf16[256,768]{1,0:T(8,128)(2,1)} %get-tuple-element.20), channel_id=1, source_target_pairs={{0,1},{1,0},{2,3},{3,2},{4,5},{5,4},{6,7},{7,6},{8,9},{9,8},{10,11... | collective-permute-start | bytes 1179656 | tf_op jit(solution)/shard_map/ppermute | solution.py:293
  40.9 6.1 %collective-permute-start.7 = (bf16[128,512]{1,0:T(8,128)(2,1)S(1)}, bf16[128,512]{1,0:T(8,128)(2,1)S(1)}, u32[]{:S(2)}, u32[]{:S(2)}) collective-permute-start(bf16[128,512]{1,0:T(8,128)(2,1)S(1)} %shard_map.116.p0), channel_id=1, source_target_pairs={{0,192},{64,128},{128,64},{192,0},{1,193},{65,129},{129,65},{193,1... | collective-permute-start | bytes 393224 | tf_op jit(solution)/shard_map/ppermute | solution.py:335
  43.7 5.3 %collective-permute-start.6 = (bf16[128,512]{1,0:T(8,128)(2,1)S(1)}, bf16[128,512]{1,0:T(8,128)(2,1)S(1)}, u32[]{:S(2)}, u32[]{:S(2)}) collective-permute-start(bf16[128,512]{1,0:T(8,128)(2,1)S(1)} %shard_map.116.p0), channel_id=1, source_target_pairs={{0,128},{64,192},{128,0},{192,64},{1,129},{65,193},{129,1},{193,65... | collective-permute-start | bytes 393224 | tf_op jit(solution)/shard_map/ppermute | solution.py:335
  44.0 5.0 %collective-permute-start.5 = (bf16[128,512]{1,0:T(8,128)(2,1)S(1)}, bf16[128,512]{1,0:T(8,128)(2,1)S(1)}, u32[]{:S(2)}, u32[]{:S(2)}) collective-permute-start(bf16[128,512]{1,0:T(8,128)(2,1)S(1)} %shard_map.116.p0), channel_id=1, source_target_pairs={{0,64},{64,0},{128,192},{192,128},{1,65},{65,1},{129,193},{193,129... | collective-permute-start | bytes 393224 | tf_op jit(solution)/shard_map/ppermute | solution.py:335
  49.0 0.9 copy-start.3
  49.9 0.9 copy-start.4
  50.9 0.9 copy-start.5
  51.8 0.9 copy-start.6
  77.8 5.4 %collective-permute-start.11 = (bf16[128,512]{1,0:T(8,128)(2,1)S(1)}, bf16[128,512]{1,0:T(8,128)(2,1)S(1)}, u32[]{:S(2)}, u32[]{:S(2)}) collective-permute-start(bf16[128,512]{1,0:T(8,128)(2,1)S(1)} %shard_map.119.refs_0_), channel_id=1, source_target_pairs={{0,192},{64,128},{128,64},{192,0},{1,193},{65,129},{129,65},{193,1... | collective-permute-start | bytes 393224 | tf_op jit(solution)/shard_map/ppermute | solution.py:335
  79.6 5.3 %collective-permute-start.10 = (bf16[128,512]{1,0:T(8,128)(2,1)S(1)}, bf16[128,512]{1,0:T(8,128)(2,1)S(1)}, u32[]{:S(2)}, u32[]{:S(2)}) collective-permute-start(bf16[128,512]{1,0:T(8,128)(2,1)S(1)} %shard_map.119.refs_0_), channel_id=1, source_target_pairs={{0,128},{64,192},{128,0},{192,64},{1,129},{65,193},{129,1},{193,65... | collective-permute-start | bytes 393224 | tf_op jit(solution)/shard_map/ppermute | solution.py:335
  80.2 4.7 %collective-permute-start.9 = (bf16[128,512]{1,0:T(8,128)(2,1)S(1)}, bf16[128,512]{1,0:T(8,128)(2,1)S(1)}, u32[]{:S(2)}, u32[]{:S(2)}) collective-permute-start(bf16[128,512]{1,0:T(8,128)(2,1)S(1)} %shard_map.119.refs_0_), channel_id=1, source_target_pairs={{0,64},{64,0},{128,192},{192,128},{1,65},{65,1},{129,193},{193,129... | collective-permute-start | bytes 393224 | tf_op jit(solution)/shard_map/ppermute | solution.py:335
  85.0 12.2 %collective-permute-start.12 = (bf16[128,256]{1,0:T(8,128)(2,1)S(1)}, bf16[128,256]{1,0:T(8,128)(2,1)S(1)}, u32[]{:S(2)}, u32[]{:S(2)}) collective-permute-start(bf16[128,256]{1,0:T(8,128)(2,1)S(1)} %get-tuple-element.25), channel_id=1, source_target_pairs={{0,1},{1,0},{2,3},{3,2},{4,5},{5,4},{6,7},{7,6},{8,9},{9,8},{10,11... | collective-permute-start | bytes 196616 | tf_op jit(solution)/shard_map/ppermute | solution.py:293
